TPU v7x, 32 devices: a whole 2x2x4 slice. The times are simulated.
32 devices in a mesh: sp: 16 (over z, y, x), tp: 2 (over core).
Axes of the slice: x: 2, y: 2, z: 4, core: 2. Of those that a mesh axis runs over, the one named last changes fastest.
Arguments:
- x_rows: bfloat16 [2048, 2048], P('sp'), may hold values from -6 to 6
- queries: bfloat16 [2048, 1024], P('sp', 'tp'), may hold values from -8 to 8
- keys: bfloat16 [2048, 512], P('sp', 'tp'), may hold values from -8 to 8
- values: bfloat16 [2048, 512], P('sp', 'tp'), may hold values from -6 to 6
- query_norm_gain: float32 [64], replicated, may hold values from 1 to 8
- key_norm_gain: float32 [64], replicated, may hold values from 1 to 8
- out_weight: bfloat16 [1024, 2048], P('tp'), may hold values from -0.1875 to 0.1875
- ffn_gain: float32 [2048], replicated, may hold values from 0.1 to 1.9
- gate_weight: bfloat16 [2048, 5120], P('sp', 'tp'), may hold values from -0.125 to 0.125
- value_weight: bfloat16 [2048, 5120], P('sp', 'tp'), may hold values from -0.125 to 0.125
- conv_gate: float32 [3, 5120], P(None, 'tp'), may hold values from -3.5 to 3.5
- conv_value: float32 [3, 5120], P(None, 'tp'), may hold values from -3.5 to 3.5
- down_weight: bfloat16 [2048, 5120], P('sp', 'tp'), may hold values from -0.078125 to 0.078125
Outputs:
- layer_out: bfloat16 [2048, 2048], P('sp')
All inputs are finite; a program needn't handle non-finite values.
Results may differ from a plain program's by a relative error of at most 0.017.
Values may be sent and summed in bfloat16 or wider, within the bound.
A program may use at most 64 MiB of HBM per device.

v0:
```python
import functools
import math

import jax
import jax.numpy as jnp
from jax import lax
from jax.experimental import pallas as pl
from jax.experimental.pallas import tpu as pltpu
from jax.sharding import PartitionSpec as P

HEAD_SIZE = 64
GRID_ROW_WIDTH = 64


eps_norm = 1e-06
theta = 10000.0


def with_halo(cells, sides, width):
    for axis, dim in sides:
        count = lax.axis_size(axis)
        ends = count - 1
        head = lax.slice_in_dim(cells, 0, width, axis=dim)
        tail = lax.slice_in_dim(cells, cells.shape[dim] - width, cells.shape[dim], axis=dim)
        cells = jnp.concatenate(
            [
                lax.ppermute(tail, axis, [(i, (i + 1) % count) for i in range(ends)]),
                cells,
                lax.ppermute(head, axis, [((i + 1) % count, i) for i in range(ends)]),
            ],
            axis=dim,
        )
    return cells


def per_head_norm(head_block, gain_vec):
    wide_vals = head_block.astype(jnp.float32)
    inverse_rms = lax.rsqrt(jnp.mean(wide_vals * wide_vals, axis=-1, keepdims=True) + eps_norm)
    return wide_vals * inverse_rms * gain_vec


def turn_half(half_vec, places):
    quarter_len = half_vec.shape[-1] // 2
    inverse_rates = 1.0 / theta ** (
        jnp.arange(quarter_len, dtype=jnp.float32) * 2.0 / half_vec.shape[-1]
    )
    angles = places.astype(jnp.float32)[:, None] * inverse_rates[None, :]
    angles = jnp.concatenate([angles, angles], axis=-1)[:, None, :]
    front_part = half_vec[..., :quarter_len]
    back_part = half_vec[..., quarter_len:]
    return half_vec * jnp.cos(angles) + jnp.concatenate(
        [-back_part, front_part], axis=-1
    ) * jnp.sin(angles)


def apply_rotary(normed_heads, token_positions):
    half_point = normed_heads.shape[-1] // 2
    grid_row = token_positions // GRID_ROW_WIDTH
    grid_col = token_positions % GRID_ROW_WIDTH
    return jnp.concatenate(
        [
            turn_half(normed_heads[..., :half_point], grid_row),
            turn_half(normed_heads[..., half_point:], grid_col),
        ],
        axis=-1,
    )


def row_norm(rows_wide, gain_vec):
    inverse_rms = lax.rsqrt(jnp.mean(rows_wide * rows_wide, axis=-1, keepdims=True) + eps_norm)
    return (rows_wide * inverse_rms * gain_vec).astype(jnp.bfloat16)


def contract_units(left_rows, right_rows):
    return lax.dot_general(
        left_rows, right_rows, (((1,), (1,)), ((), ())), preferred_element_type=jnp.float32
    )


def shards(
    x_rows,
    queries,
    keys,
    values,
    query_norm_gain,
    key_norm_gain,
    out_weight,
    ffn_gain,
    gate_weight,
    value_weight,
    conv_gate,
    conv_value,
    down_weight,
):
    collected = (
        lax.all_gather(gate_weight, "sp", axis=0, tiled=True),
        lax.all_gather(value_weight, "sp", axis=0, tiled=True),
        lax.all_gather(down_weight, "sp", axis=0, tiled=True),
    )
    tokens_here = queries.shape[0]
    query_heads = queries.shape[1] // HEAD_SIZE
    key_heads = keys.shape[1] // HEAD_SIZE
    group_width = query_heads // key_heads
    lane_rows = group_width * tokens_here
    token_positions = lax.axis_index("sp") * tokens_here + jnp.arange(tokens_here, dtype=jnp.int32)
    rotated_queries = apply_rotary(
        per_head_norm(queries.reshape(tokens_here, query_heads, HEAD_SIZE), query_norm_gain),
        token_positions,
    )
    query_lanes = rotated_queries.reshape(tokens_here, key_heads, group_width, HEAD_SIZE).transpose(
        1, 2, 0, 3
    )
    query_lanes = query_lanes.reshape(key_heads, lane_rows, HEAD_SIZE) * HEAD_SIZE ** (-0.5)
    start_state = (
        jnp.full((key_heads, lane_rows), -1e30, jnp.float32),
        jnp.zeros((key_heads, lane_rows), jnp.float32),
        jnp.zeros((key_heads, lane_rows, HEAD_SIZE), jnp.float32),
    )
    key_piece = lax.all_gather(keys, "sp", axis=0, tiled=True)
    value_piece = lax.all_gather(values, "sp", axis=0, tiled=True)
    row_count = key_piece.shape[0]
    key_places = jnp.arange(row_count, dtype=jnp.int32)
    turned = apply_rotary(
        per_head_norm(key_piece.reshape(row_count, key_heads, HEAD_SIZE), key_norm_gain), key_places
    )
    key_span = math.gcd(row_count, 2048)
    span_count = row_count // key_span
    turned = turned.reshape(span_count, key_span, key_heads, HEAD_SIZE)
    value_matrix = value_piece.reshape(span_count, key_span, key_heads, HEAD_SIZE)

    def one_span(state_now, inputs):
        running_top, denominator, weighted = state_now
        key_block, value_block = inputs
        scores = jnp.einsum("hrd,shd->hrs", query_lanes, key_block, precision=lax.Precision.HIGHEST)
        new_top = jnp.maximum(running_top, jnp.max(scores, axis=-1))
        factor = jnp.exp(running_top - new_top)
        weights = jnp.exp(scores - new_top[..., None])
        denominator = denominator * factor + jnp.sum(weights, axis=-1)
        weighted = weighted * factor[..., None] + jnp.einsum(
            "hrs,shd->hrd",
            weights.astype(jnp.bfloat16),
            value_block,
            preferred_element_type=jnp.float32,
        )
        return ((new_top, denominator, weighted), None)

    folded_state, _ = lax.scan(one_span, start_state, (turned, value_matrix))
    running_top, denominator, weighted = folded_state
    attended = (weighted / denominator[..., None]).reshape(
        key_heads, group_width, tokens_here, HEAD_SIZE
    )
    attended = (
        attended.transpose(2, 0, 1, 3)
        .reshape(tokens_here, query_heads * HEAD_SIZE)
        .astype(jnp.bfloat16)
    )
    share_rows = tokens_here // lax.axis_size("tp")
    head_share = lax.psum_scatter(
        jnp.dot(attended, out_weight, preferred_element_type=jnp.float32).astype(jnp.bfloat16),
        "tp",
        scatter_dimension=0,
        tiled=True,
    ).astype(jnp.float32)
    own_rows = lax.dynamic_slice_in_dim(x_rows, lax.axis_index("tp") * share_rows, share_rows, 0)
    middle_rows = own_rows.astype(jnp.float32) + head_share
    normed = lax.all_gather(row_norm(middle_rows, ffn_gain), "tp", axis=0, tiled=True)
    unit_local = gate_weight.shape[1]
    gate_pre = jnp.dot(normed, collected[0], preferred_element_type=jnp.float32).astype(
        jnp.bfloat16
    )
    value_pre = jnp.dot(normed, collected[1], preferred_element_type=jnp.float32).astype(
        jnp.bfloat16
    )
    joined = jnp.concatenate([gate_pre, value_pre], axis=1)
    padded = with_halo(joined, (("sp", 0),), 1).astype(jnp.float32)
    conv_taps = jnp.concatenate([conv_gate, conv_value], axis=1)
    convolved = conv_taps[0] * padded[:-2] + conv_taps[1] * padded[1:-1] + conv_taps[2] * padded[2:]
    hidden = (jax.nn.silu(convolved[:, :unit_local]) * convolved[:, unit_local:]).astype(
        jnp.bfloat16
    )
    unit_share = lax.psum_scatter(
        contract_units(hidden, collected[2]).astype(jnp.bfloat16),
        "tp",
        scatter_dimension=0,
        tiled=True,
    ).astype(jnp.float32)
    finished = (middle_rows + unit_share).astype(jnp.bfloat16)
    return lax.all_gather(finished, "tp", axis=0, tiled=True)

LANES = 128
MESH = pl.DeviceIdType.MESH
BF = jnp.bfloat16
F32 = jnp.float32


def rem(a, b):
    return a % b if isinstance(a, int) else lax.rem(a, b)


def nt(left, right):
    return lax.dot_general(left, right, (((1,), (1,)), ((), ())), preferred_element_type=F32)


def layer_kernel(
    n, x_ref, q_ref, kv_ref, qg_ref, kg_ref, cos_ref, sin_ref, wo_ref, fg_ref, w_ref,
    cg_ref, cv_ref, out_ref,
    wo_buf, kvbuf, qbuf, kcat, qcat, att_s, attbuf, po_s, po_r, mid, allnorm, edge_s, edge_r, wrecv,
    pre_g, pre_v, part, ddbuf, own_sum, rs_s, rs_r, fin_s, fin_r,
    loc, kv_ss, kv_rs, q_ss, q_rs, w_ss, w_rs, wf_ss, wf_rs, dw_ss, dw_rs, df_ss, df_rs, o_ss, o_rs, po_sem, ag_ss, ag_rs, fw_ss, fw_rs,
    ch_ss, ch_rs, h_sem, dd_ss, dd_rs, c_ss, c_rs, fin_sem,
):
    sp = lax.axis_index("sp")
    core = lax.axis_index("tp")
    mate = 1 - core
    rows = x_ref.shape[0]
    half_rows = rows // 2
    width = x_ref.shape[1]
    kv_heads = kv_ref.shape[1] // LANES
    plane = n // 4
    group = 2 * plane
    tokens = n * rows
    q_tokens = kv_heads * rows
    units = w_ref.shape[1] // 3
    head_at = rem(sp, kv_heads)
    q_base = sp - head_at
    place = rem(sp, plane)
    side = rem(sp // plane, 2)
    wing = sp // (2 * plane)
    member = wing * plane + place

    def chip(m, at_side):
        return (m // plane) * (2 * plane) + at_side * plane + rem(m, plane)

    def ahead(d):
        return rem(wing + d // plane, 2) * plane + rem(place + rem(d, plane), plane)

    def behind(d):
        return rem(wing + d // plane, 2) * plane + rem(
            place + plane - rem(d, plane), plane
        )

    twin = chip(member, 1 - side)

    def remote(src, dst, ss, rs, device):
        return pltpu.make_async_remote_copy(
            src_ref=src, dst_ref=dst, send_sem=ss, recv_sem=rs, device_id=device, device_id_type=MESH
        )

    def lane_block(k):
        return pl.ds(pl.multiple_of(k * LANES, LANES), LANES)

    def span(start, size, unit):
        return pl.ds(pl.multiple_of(start, unit), size)

    def loop(lo, hi, fn):
        def step(k, carry):
            fn(k)
            return carry

        lax.fori_loop(lo, hi, step, 0)

    barrier = pltpu.get_barrier_semaphore()

    def greet(d):
        t = rem(sp + d, n)
        pl.semaphore_signal(barrier, inc=1, device_id=(t, core), device_id_type=MESH)

    loop(1, n, greet)
    pl.semaphore_signal(barrier, inc=1, device_id=(sp, mate), device_id_type=MESH)
    pl.semaphore_wait(barrier, n)

    def q_copy(d):
        t = q_base + rem(head_at + d, kv_heads)
        return remote(
            q_ref.at[:, lane_block(t - q_base)], qbuf.at[span(head_at * rows, rows, rows)],
            q_ss.at[d], q_rs.at[d], (t, core),
        )

    def kv_copy(d):
        t = rem(sp + d, n)
        return remote(
            kv_ref.at[:, lane_block(rem(t, kv_heads))], kvbuf.at[span(sp * rows, rows, rows)],
            kv_ss.at[d], kv_rs.at[d], (t, core),
        )

    up_part, down_part = slice(0, 2 * units), slice(2 * units, 3 * units)

    def w_copy(d, part_at, ss, rs):
        m = ahead(d)
        return remote(
            w_ref.at[m, part_at], wrecv.at[part_at, lane_block(sp)],
            ss.at[d], rs.at[d], (chip(m, side), core),
        )

    def twin_first(part_at, ss, rs):
        return remote(
            w_ref.at[member, part_at], wrecv.at[part_at, lane_block(sp)],
            ss.at[0], rs.at[0], (twin, core),
        )

    def twin_copy(d, part_at, ss, rs):
        at = wrecv.at[part_at, lane_block(chip(behind(d), side))]
        return remote(at, at, ss.at[d], rs.at[d], (twin, core))

    def pass_on(d, part_at, ss, rs, next_ss, next_rs):
        dst = wrecv.at[part_at, lane_block(chip(behind(d), side))]
        remote(dst, dst, ss.at[d], rs.at[d], (twin, core)).wait_recv()
        twin_copy(d, part_at, next_ss, next_rs).start()

    def twin_wait(d, part_at, ss, rs):
        dst = wrecv.at[part_at, lane_block(chip(behind(d), 1 - side))]
        remote(dst, dst, ss.at[d], rs.at[d], (twin, core)).wait_recv()

    later = plane + plane // 2
    gate_sems, gate_next = (w_ss, w_rs), (wf_ss, wf_rs)
    down_sems, down_next = (dw_ss, dw_rs), (df_ss, df_rs)

    own_q = pltpu.make_async_copy(
        q_ref.at[:, lane_block(head_at)], qbuf.at[span(head_at * rows, rows, rows)], loc.at[0]
    )
    own_kv = pltpu.make_async_copy(
        kv_ref.at[:, lane_block(head_at)], kvbuf.at[span(sp * rows, rows, rows)], loc.at[1]
    )
    own_w = pltpu.make_async_copy(w_ref.at[member], wrecv.at[:, lane_block(sp)], loc.at[2])
    own_q.start()
    wo_copy = pltpu.make_async_copy(wo_ref, wo_buf, loc.at[3])
    wo_copy.start()
    own_kv.start()
    loop(1, kv_heads, lambda d: q_copy(d).start())
    loop(1, n, lambda d: kv_copy(d).start())
    loop(1, plane, lambda d: w_copy(d, up_part, *gate_sems).start())
    loop(1, plane, lambda d: w_copy(d, down_part, *down_sems).start())
    own_w.start()

    lane = lax.broadcasted_iota(jnp.int32, (GRID_ROW_WIDTH, LANES), 1)
    low = lane < HEAD_SIZE
    first = rem(lane, 2 * HEAD_SIZE // 4) < HEAD_SIZE // 4
    by_row = rem(lane, HEAD_SIZE) < HEAD_SIZE // 2

    def turn(vals, grid_row):
        cos = jnp.where(by_row, cos_ref[pl.ds(grid_row, 1), :], cos_ref[:GRID_ROW_WIDTH, :])
        sin = jnp.where(by_row, sin_ref[pl.ds(grid_row, 1), :], sin_ref[:GRID_ROW_WIDTH, :])
        quarter = HEAD_SIZE // 4
        swapped = jnp.where(
            first, pltpu.roll(vals, LANES - quarter, 1), pltpu.roll(vals, quarter, 1)
        )
        return vals * cos + swapped * sin

    q_gain = jnp.concatenate([qg_ref[...]] * 2, axis=1)
    k_gain = jnp.concatenate([kg_ref[...]] * 2, axis=1)

    def split(vals):
        top = vals.astype(BF).astype(F32)
        return top, (vals - top).astype(BF).astype(F32)

    def make_q(r):
        at = span(r * GRID_ROW_WIDTH, GRID_ROW_WIDTH, GRID_ROW_WIDTH)
        vals = qbuf[at, :].astype(F32)
        sq = vals * vals
        low_sum = jnp.sum(jnp.where(low, sq, 0.0), axis=1, keepdims=True)
        high_sum = jnp.sum(jnp.where(low, 0.0, sq), axis=1, keepdims=True)
        inverse = jnp.where(
            low,
            lax.rsqrt(low_sum * (1.0 / HEAD_SIZE) + eps_norm),
            lax.rsqrt(high_sum * (1.0 / HEAD_SIZE) + eps_norm),
        )
        turned = turn(vals * inverse * q_gain, q_base * (rows // GRID_ROW_WIDTH) + r)
        top, rest = split(turned * HEAD_SIZE ** (-0.5))
        qcat[at, :] = jnp.where(low, top, pltpu.roll(rest, HEAD_SIZE, 1)).astype(BF)
        later = span(q_tokens + r * GRID_ROW_WIDTH, GRID_ROW_WIDTH, GRID_ROW_WIDTH)
        qcat[later, :] = jnp.where(low, pltpu.roll(top, HEAD_SIZE, 1), rest).astype(BF)

    own_q.wait()

    def q_take(d):
        s = rem(head_at + kv_heads - d, kv_heads)
        dst = qbuf.at[span(s * rows, rows, rows)]

        @pl.when(d > 0)
        def _():
            remote(dst, dst, q_ss.at[d], q_rs.at[d], (q_base + s, core)).wait_recv()

        for r in range(rows // GRID_ROW_WIDTH):
            make_q(s * (rows // GRID_ROW_WIDTH) + r)

    loop(0, kv_heads, q_take)
    twin_first(up_part, *gate_next).start()
    loop(plane, later, lambda d: w_copy(d, up_part, *gate_sems).start())
    steps = rows // GRID_ROW_WIDTH

    def make_k(r):
        at = span(r * GRID_ROW_WIDTH, GRID_ROW_WIDTH, GRID_ROW_WIDTH)
        vals = kvbuf[at, :].astype(F32)
        total = jnp.sum(jnp.where(low, vals * vals, 0.0), axis=1, keepdims=True)
        turned = turn(
            vals * lax.rsqrt(total * (1.0 / HEAD_SIZE) + eps_norm) * k_gain, r
        )
        top, rest = split(turned)
        kcat[at, :LANES] = jnp.where(low, top, pltpu.roll(top, HEAD_SIZE, 1)).astype(BF)
        kcat[at, LANES:] = jnp.where(low, rest, pltpu.roll(rest, HEAD_SIZE, 1)).astype(BF)

    own_kv.wait()

    def kv_take(d):
        s = rem(sp + n - d, n)
        dst = kvbuf.at[span(s * rows, rows, rows)]

        @pl.when(d > 0)
        def _():
            remote(dst, dst, kv_ss.at[d], kv_rs.at[d], (s, core)).wait_recv()

        for r in range(steps):
            make_k(s * steps + r)

    loop(0, n, kv_take)
    loop(1, plane, lambda d: pass_on(d, up_part, *gate_sems, *gate_next))

    def o_copy(d):
        k = rem(head_at + d, kv_heads)
        return remote(
            att_s.at[span(k * rows, rows, rows)], attbuf.at[:, lane_block(head_at)],
            o_ss.at[d], o_rs.at[d], (q_base + k, core),
        )

    low_rows = lax.broadcasted_iota(jnp.int32, (rows, LANES), 1) < HEAD_SIZE

    def attend(k):
        both = jnp.concatenate(
            [qcat[span(k * rows, rows, rows), :], qcat[span(q_tokens + k * rows, rows, rows), :]],
            axis=0,
        )
        scores = nt(jnp.concatenate([both, both], axis=1), kcat[...])
        shifted = jnp.exp(scores - jnp.max(scores, axis=1, keepdims=True))
        total = jnp.sum(shifted, axis=1, keepdims=True)
        summed = jnp.dot(shifted.astype(BF), kvbuf[...], preferred_element_type=F32) / total
        return jnp.where(
            low_rows, pltpu.roll(summed[:rows], HEAD_SIZE, 1), summed[rows:]
        ).astype(BF)

    def attend_send(d):
        k = rem(head_at + d, kv_heads)
        att_s[span(k * rows, rows, rows), :] = attend(k)

        @pl.when(d < kv_heads)
        def _():
            o_copy(d).start()

    loop(1, kv_heads + 1, attend_send)
    attbuf[:, lane_block(head_at)] = att_s[span(head_at * rows, rows, rows), :]

    def o_wait(d):
        s = rem(head_at + kv_heads - d, kv_heads)
        dst = attbuf.at[:, lane_block(s)]
        remote(dst, dst, o_ss.at[d], o_rs.at[d], (q_base + s, core)).wait_recv()

    loop(1, kv_heads, o_wait)

    wo_copy.wait()
    po_s[...] = jnp.dot(attbuf[...], wo_buf[...], preferred_element_type=F32).astype(BF)
    po_copy = remote(
        po_s.at[span(mate * half_rows, half_rows, half_rows)], po_r, po_sem.at[0], po_sem.at[1],
        (sp, mate),
    )
    po_copy.start()
    mine = span(core * half_rows, half_rows, half_rows)
    base = x_ref[mine, :].astype(F32) + po_s[mine, :].astype(F32)
    po_copy.wait_recv()
    middle = base + po_r[...].astype(F32)
    mid[...] = middle
    scaled = lax.rsqrt(jnp.mean(middle * middle, axis=1, keepdims=True) + eps_norm)
    normed = (middle * scaled * fg_ref[...]).astype(BF)

    def slot(k, c):
        return allnorm.at[span(k * rows + c * half_rows, half_rows, half_rows)]

    allnorm[span(member * rows + core * half_rows, half_rows, half_rows), :] = normed

    def ag_copy(d):
        to = ahead(rem(d, plane)) if d != plane else ahead(d)
        of = member if d <= plane else (1 - wing) * plane + place
        return remote(
            slot(of, core), slot(of, core), ag_ss.at[d], ag_rs.at[d], (chip(to, side), core)
        )

    def fw_copy(d):
        s = behind(d)
        return remote(slot(s, core), slot(s, core), fw_ss.at[d], fw_rs.at[d], (sp, mate))

    def ag_wait(d):
        s = behind(d)
        remote(slot(s, core), slot(s, core), ag_ss.at[d], ag_rs.at[d], (sp, mate)).wait_recv()
        fw_copy(d).start()

    ag_copy(plane).start()
    for d in range(1, plane):
        ag_copy(d).start()
    fw_copy(0).start()

    own_w.wait()
    loop(later, group, lambda d: w_copy(d, up_part, *gate_sems).start())
    twin_first(down_part, *down_next).start()
    loop(1, plane, lambda d: pass_on(d, down_part, *down_sems, *down_next))
    loop(plane, later, lambda d: pass_on(d, up_part, *gate_sems, *gate_next))
    ag_wait(plane)
    for d in range(plane + 1, group):
        ag_copy(d).start()
    loop(plane, group, lambda d: w_copy(d, down_part, *down_sems).start())
    loop(later, group, lambda d: pass_on(d, up_part, *gate_sems, *gate_next))

    def up(block):
        both = nt(block, wrecv[: 2 * units, :]).astype(BF).astype(F32)
        return both[:, :units], both[:, units:]

    seg = plane * rows
    pitch = seg + 16

    def row_of(m):
        return (m // plane) * pitch + rem(m, plane) * rows

    def take(d):
        @pl.when(jnp.logical_and(d > 0, d != plane))
        def _():
            ag_wait(d)

    def mate_wait(d):
        s = behind(d)
        remote(slot(s, mate), slot(s, mate), fw_ss.at[d], fw_rs.at[d], (sp, mate)).wait_recv()

    def up_rows(k):
        side_at = rem(wing + k, 2)
        loop(k * plane, (k + 1) * plane, mate_wait)
        gate, value = up(allnorm[span(side_at * seg, seg, rows), :])
        at = span(side_at * pitch + 8, seg, 8)
        pre_g[at, :] = gate
        pre_v[at, :] = value

    loop(0, group, take)
    loop(0, group, lambda d: twin_wait(d, up_part, *gate_next))
    loop(plane, group, lambda d: pass_on(d, down_part, *down_sems, *down_next))
    loop(0, 2, up_rows)

    edge_at = (8, 8 + seg - 1, pitch + 8, pitch + 8 + seg - 1)
    edge_s[...] = jnp.concatenate(
        [
            jnp.concatenate([pre[k : k + 1, :] for k in edge_at] * 2, axis=0)
            for pre in (pre_g, pre_v)
        ],
        axis=0,
    )
    edge_copy = remote(edge_s, edge_r, h_sem.at[0], h_sem.at[1], (twin, core))
    edge_copy.start()
    loop(0, group, lambda d: twin_wait(d, down_part, *down_next))
    edge_copy.wait_recv()
    for pre, first_row in ((pre_g, 0), (pre_v, 8)):
        near = [
            jnp.broadcast_to(edge_r[first_row + k : first_row + k + 1, :], (8, units))
            for k in range(4)
        ]
        none = jnp.zeros((8, units), F32)
        pre[0:8, :] = jnp.where(side == 0, none, near[1])
        pre[8 + seg : pitch, :] = jnp.where(side == 0, near[0], near[2])
        pre[pitch : pitch + 8, :] = jnp.where(side == 0, near[1], near[3])
        pre[pitch + 8 + seg :, :] = jnp.where(side == 0, near[2], none)

    def convolve(ref, taps, k):
        block = ref[span(row_of(k), rows + 16, 8), :]
        return (
            taps[0:1, :] * block[7 : 7 + rows]
            + taps[1:2, :] * block[8 : 8 + rows]
            + taps[2:3, :] * block[9 : 9 + rows]
        )

    def dd_copy(d):
        return remote(
            part.at[d, span(mate * half_rows, half_rows, half_rows)], ddbuf.at[d],
            dd_ss.at[d], dd_rs.at[d], (sp, mate),
        )

    def c_copy(d, to):
        return remote(rs_s.at[d], rs_r.at[d], c_ss.at[d], c_rs.at[d], (chip(to, side), core))

    def c_near(d):
        return c_copy(d, ahead(rem(d, plane)))

    quarter_rows = half_rows // 2

    def c_half(d, h, to):
        at = span(h * quarter_rows, quarter_rows, quarter_rows)
        return remote(
            rs_s.at[d, at], rs_r.at[d, at], ch_ss.at[2 * d + h], ch_rs.at[2 * d + h],
            (chip(to, side), core),
        )

    def c_cross(d, h):
        return c_half(d, h, ahead(rem(d, plane)))

    def combine(d):
        dd_copy(d).wait_recv()
        return part[d, mine, :].astype(F32) + ddbuf[d].astype(F32)

    def send_sum(d):
        rs_s[d] = combine(d).astype(BF)

        @pl.when(d < plane)
        def _():
            c_near(d).start()

        @pl.when(d > plane)
        def _():
            c_cross(d, 0).start()

    def order(j):
        return plane * (1 - j // plane) + rem(j + 1, plane)

    def down(j):
        d = order(j)
        k = ahead(d)
        gate = convolve(pre_g, cg_ref, k)
        value = convolve(pre_v, cv_ref, k)
        hidden = (gate / (1.0 + jnp.exp(-gate)) * value).astype(BF)
        part[d] = jnp.dot(hidden, wrecv[2 * units :, :], preferred_element_type=F32).astype(BF)
        dd_copy(d).start()
        last = order(jnp.maximum(j - 1, 0))

        @pl.when(jnp.logical_and(j > 0, rem(last, plane) > 0))
        def _():
            send_sum(last)

        @pl.when(j == plane)
        def _():
            loop(plane + 1, group, lambda k: c_cross(k, 1).start())

    loop(0, group, down)

    def add_in(d):
        remote(rs_r.at[d], rs_r.at[d], c_ss.at[d], c_rs.at[d], (sp, mate)).wait_recv()
        own_sum[...] = own_sum[...] + rs_r[d].astype(F32)

    own_sum[...] = combine(plane)
    far = (1 - wing) * plane + place

    def far_send(h):
        at = span(h * quarter_rows, quarter_rows, quarter_rows)

        def half_in(d):
            c_cross(d, h).wait_recv()
            own_sum[at, :] = own_sum[at, :] + rs_r[d, at, :].astype(F32)

        loop(plane + 1, group, half_in)
        rs_s[plane, at, :] = own_sum[at, :].astype(BF)
        c_half(plane, h, far).start()

    loop(0, 2, far_send)
    own_sum[...] = mid[...] + combine(0)
    loop(1, plane, add_in)

    def far_take(h):
        at = span(h * quarter_rows, quarter_rows, quarter_rows)
        c_half(plane, h, far).wait_recv()
        own_sum[at, :] = own_sum[at, :] + rs_r[plane, at, :].astype(F32)

    loop(0, 2, far_take)
    fin_s[...] = own_sum[...].astype(BF)
    fin_copy = remote(fin_s, fin_r, fin_sem.at[0], fin_sem.at[1], (sp, mate))
    fin_copy.start()
    out_ref[mine, :] = fin_s[...]

    loop(1, kv_heads, lambda d: q_copy(d).wait_send())
    loop(1, n, lambda d: kv_copy(d).wait_send())
    loop(1, group, lambda d: w_copy(d, up_part, *gate_sems).wait_send())
    loop(1, group, lambda d: w_copy(d, down_part, *down_sems).wait_send())
    loop(0, group, lambda d: twin_copy(d, up_part, *gate_next).wait_send())
    loop(0, group, lambda d: twin_copy(d, down_part, *down_next).wait_send())
    loop(1, kv_heads, lambda d: o_copy(d).wait_send())
    po_copy.wait_send()
    for d in range(1, group):
        ag_copy(d).wait_send()
    loop(0, group, lambda d: fw_copy(d).wait_send())
    edge_copy.wait_send()
    loop(0, group, lambda d: dd_copy(d).wait_send())
    loop(1, plane, lambda d: c_near(d).wait_send())
    for h in range(2):
        for d in range(plane + 1, group):
            c_cross(d, h).wait_send()
        c_half(plane, h, far).wait_send()
    fin_copy.wait_send()
    fin_copy.wait_recv()
    out_ref[span(mate * half_rows, half_rows, half_rows), :] = fin_r[...]


def rotary_tables(count):
    lanes = jnp.arange(LANES)
    length = HEAD_SIZE // 2
    rate_at = (lanes % (length // 2)).astype(F32)
    rates = 1.0 / theta ** (rate_at * 2.0 / length)
    angles = jnp.arange(count, dtype=F32)[:, None] * rates[None, :]
    sign = jnp.where(lanes % length < length // 2, -1.0, 1.0)
    return jnp.cos(angles), jnp.sin(angles) * sign[None, :]


def kernel_shards(
    n, x_rows, queries, keys, values, query_norm_gain, key_norm_gain, out_weight, ffn_gain,
    gate_weight, value_weight, conv_gate, conv_value, down_weight,
):
    rows, width = x_rows.shape
    kv_heads = keys.shape[1] // HEAD_SIZE
    plane = n // 4
    group = 2 * plane
    unit_local = gate_weight.shape[1]
    units = unit_local // group
    depth = gate_weight.shape[0]
    kv = jnp.concatenate(
        [keys.reshape(rows, kv_heads, HEAD_SIZE), values.reshape(rows, kv_heads, HEAD_SIZE)], axis=-1
    ).reshape(rows, kv_heads * LANES)
    turned = [
        w.T.reshape(group, units, depth) for w in (gate_weight, value_weight, down_weight)
    ]
    weights = jnp.concatenate(turned, axis=1)
    at = lax.axis_index("sp")
    chip = (at // group) * plane + rem(at, plane)
    taps = [lax.dynamic_slice_in_dim(t, chip * units, units, 1) for t in (conv_gate, conv_value)]
    cos, sin = rotary_tables(max(GRID_ROW_WIDTH, n * rows // GRID_ROW_WIDTH))
    tokens, q_tokens, span_rows = n * rows, kv_heads * rows, group * rows
    half_rows = rows // 2
    dma = pltpu.SemaphoreType.DMA
    vm = pltpu.VMEM
    scratch = [
        vm(out_weight.shape, BF), vm((tokens, LANES), BF), vm((q_tokens, LANES), BF), vm((tokens, 2 * LANES), BF),
        vm((2 * q_tokens, LANES), BF), vm((q_tokens, LANES), BF), vm((rows, kv_heads * LANES), BF),
        vm((rows, width), BF), vm((half_rows, width), BF), vm((half_rows, width), F32),
        vm((span_rows, width), BF), vm((16, units), F32),
        vm((16, units), F32), vm((3 * units, width), BF),
        vm((span_rows + 32, units), F32), vm((span_rows + 32, units), F32),
        vm((group, rows, width), BF), vm((group, half_rows, width), BF),
        vm((half_rows, width), F32), vm((group, half_rows, width), BF),
        vm((group, half_rows, width), BF), vm((half_rows, width), BF), vm((half_rows, width), BF),
        dma((4,)), dma((n,)), dma((n,)), dma((kv_heads,)), dma((kv_heads,)), *[dma((group,))] * 8,
        dma((kv_heads,)), dma((kv_heads,)), dma((2,)), dma((group,)), dma((group,)),
        dma((group,)), dma((group,)), dma((2 * group,)), dma((2 * group,)), dma((2,)),
        dma((group,)), dma((group,)),
        dma((group,)), dma((group,)), dma((2,)),
    ]
    args = (
        x_rows, queries, kv, query_norm_gain[None, :], key_norm_gain[None, :],
        cos, sin, out_weight, ffn_gain[None, :], weights, taps[0], taps[1],
    )
    return pl.pallas_call(
        lambda *refs: layer_kernel(n, *refs),
        out_shape=jax.ShapeDtypeStruct((rows, width), BF),
        in_specs=[
            pl.BlockSpec(memory_space=pl.ANY if a is out_weight else pltpu.VMEM) for a in args
        ],
        out_specs=pl.BlockSpec(memory_space=pltpu.VMEM),
        scratch_shapes=scratch,
        compiler_params=pltpu.CompilerParams(
            collective_id=0, has_side_effects=True, vmem_limit_bytes=60 * 2**20
        ),
        name="layer",
    )(*args)


def suits(mesh, sizes):
    n, pair = mesh.shape["sp"], mesh.shape["tp"]
    x_rows, queries, keys, gate = sizes
    if pair != 2 or n % 4:
        return False
    rows, group = x_rows[0] // n, n // 2
    heads = keys[1] // pair // HEAD_SIZE
    units = gate[1] // pair
    return (
        rows % GRID_ROW_WIDTH == 0
        and rows % 32 == 0
        and queries[1] == 2 * keys[1]
        and n % heads == 0
        and 2 * HEAD_SIZE == LANES
        and x_rows[1] == n * LANES
        and units % (16 * group) == 0
    )


def solution(mesh):
    placed = (
        P("sp", None),
        P("sp", "tp"),
        P("sp", "tp"),
        P("sp", "tp"),
        P(),
        P(),
        P("tp", None),
        P(),
        P("sp", "tp"),
        P("sp", "tp"),
        P(None, "tp"),
        P(None, "tp"),
        P("sp", "tp"),
    )
    def run(*arrays):
        n = mesh.shape["sp"]
        fits = suits(mesh, [arrays[k].shape for k in (0, 1, 2, 8)])
        local = functools.partial(kernel_shards, n) if fits else shards
        return jax.shard_map(
            local, mesh=mesh, in_specs=placed, out_specs=P("sp", None), check_vma=False
        )(*arrays)

    return run
```

profile of v0, /device:TPU:0, one launch (start us, length us, event | category | flops | bytes accessed | tf_op | source)
XLA Modules:
  0.0 129.7 jit_solution(2392821076573165866)
XLA Ops:
  0.0 0.0 copy-start
  0.0 1.4 %constant_dynamic-slice_fusion = (f32[3,320]{1,0:T(4,128)}, f32[3,320]{1,0:T(4,128)}) fusion(f32[3,2560]{1,0:T(4,128)} %param.24, s32[]{:T(128)S(6)} %select_n.41, f32[3,2560]{1,0:T(4,128)} %param.23), kind=kLoop, calls=%fused_computation.12 | loop fusion | bytes 15364 | tf_op jit(solution)/shard_map/dynamic_slice | solution.py:721
  1.5 0.8 sine_multiply_fusion
  2.2 1.4 %copy.22 = bf16[2560,128]{1,0:T(8,128)(2,1)S(1)} copy(bf16[2560,128]{0,1:T(8,128)(2,1)} %bitcast.15) | data formatting | bytes 1310720 | tf_op jit(solution)/shard_map/transpose | solution.py:716
  3.6 1.4 %copy.20 = bf16[2560,128]{1,0:T(8,128)(2,1)S(1)} copy(bf16[2560,128]{0,1:T(8,128)(2,1)} %bitcast.16) | data formatting | bytes 1310720 | tf_op jit(solution)/shard_map/transpose | solution.py:716
  5.1 0.0 copy-done
  5.1 0.3 copy.21
  5.4 0.0 copy-start.1
  5.4 0.0 copy-start.2
  5.4 1.4 %pad_maximum_fusion.refs_9_ = bf16[8,960,128]{2,1,0:T(8,128)(2,1)} fusion(bf16[8,320,128]{2,1,0:T(8,128)(2,1)S(1)} %bitcast.12, bf16[8,320,128]{2,1,0:T(8,128)(2,1)S(1)} %bitcast.14, bf16[8,320,128]{2,1,0:T(8,128)(2,1)S(1)} %bitcast.13), kind=kLoop, calls=%fused_computation | loop fusion | flops 5898240 | bytes 3932160 | tf_op jit(solution)/shard_map/concatenate | solution.py:718
  6.9 0.0 copy-done.1
  6.9 0.1 copy.17
  7.0 0.0 copy-done.2
  7.0 0.1 copy.18
  7.1 0.8 copy.23.refs_2_
  7.9 119.9 %layer.1 = bf16[128,2048]{1,0:T(8,128)(2,1)} custom-call(bf16[128,2048]{1,0:T(8,128)(2,1)} %refs_0_.1, bf16[128,512]{1,0:T(8,128)(2,1)} %refs_1_.1, bf16[128,512]{1,0:T(8,128)(2,1)} %copy.23.refs_2_, f32[1,64]{1,0:T(1,128)} %bitcast.22, f32[1,64]{1,0:T(1,128)} %bitcast.23, f32[64,128]{1,0:T(8,128)} %get-tuple-element.6.refs_5_, ...), custom_call_target="tpu_custom_call" | custom-call | tf_op jit(solution)/shard_map/layer/pallas_call | solution.py:747
  127.8 1.9 %copy.25 = bf16[128,2048]{1,0:T(8,128)(2,1)} copy(bf16[128,2048]{1,0:T(8,128)(2,1)} %layer.1) | data formatting | bytes 1048576
  (2 shorter events, 0.0 us)
Async XLA Ops:
  0.0 5.1 %copy-start = (bf16[128,2560]{1,0:T(8,128)(2,1)S(1)}, bf16[128,2560]{1,0:T(8,128)(2,1)}, u32[]{:S(2)}) copy-start(bf16[128,2560]{1,0:T(8,128)(2,1)} %param.22) | copy-start | bytes 1966084
  5.4 1.5 %copy-start.1 = (bf16[128,256]{1,0:T(8,128)(2,1)S(1)}, bf16[128,256]{1,0:T(8,128)(2,1)}, u32[]{:S(2)}) copy-start(bf16[128,256]{1,0:T(8,128)(2,1)} %param.15) | copy-start | bytes 196612
  5.4 1.6 %copy-start.2 = (bf16[128,256]{1,0:T(8,128)(2,1)S(1)}, bf16[128,256]{1,0:T(8,128)(2,1)}, u32[]{:S(2)}) copy-start(bf16[128,256]{1,0:T(8,128)(2,1)} %param.16) | copy-start | bytes 196612
where the time goes:
time: 130 us
  Pallas kernels  120 us (92%)
  local copies, waits for them, and re-layouts  7.48 us (6%)
  other arithmetic  2.22 us (2%)
    pallas_call x1, Pallas kernels, kernel_shards(): pl.pallas_call(lambda *refs: layer_kernel(n, *refs), out_shape=jax.ShapeD...  120 us
    transpose x3, local copies, waits for them, and re-layouts, kernel_shards(): w.T.reshape(group, units, depth)  3.14 us

commit v1 on v0

--- a/solution.py
+++ b/solution.py
@@ -188,6 +188,7 @@
     return lax.all_gather(finished, "tp", axis=0, tiled=True)
 
 LANES = 128
+PLANE = 4
 MESH = pl.DeviceIdType.MESH
 BF = jnp.bfloat16
 F32 = jnp.float32
@@ -195,6 +196,10 @@
 
 def rem(a, b):
     return a % b if isinstance(a, int) else lax.rem(a, b)
+
+
+def xor(a, b):
+    return rem(a + b, 2) + 2 * rem(a // 2 + b // 2, 2)
 
 
 def nt(left, right):
@@ -205,9 +210,10 @@
     n, x_ref, q_ref, kv_ref, qg_ref, kg_ref, cos_ref, sin_ref, wo_ref, fg_ref, w_ref,
     cg_ref, cv_ref, out_ref,
     wo_buf, kvbuf, qbuf, kcat, qcat, att_s, attbuf, po_s, po_r, mid, allnorm, edge_s, edge_r, wrecv,
-    pre_g, pre_v, part, ddbuf, own_sum, rs_s, rs_r, fin_s, fin_r,
-    loc, kv_ss, kv_rs, q_ss, q_rs, w_ss, w_rs, wf_ss, wf_rs, dw_ss, dw_rs, df_ss, df_rs, o_ss, o_rs, po_sem, ag_ss, ag_rs, fw_ss, fw_rs,
-    ch_ss, ch_rs, h_sem, dd_ss, dd_rs, c_ss, c_rs, fin_sem,
+    pre_g, pre_v, hid, part, ddbuf, near_s, near_r, far_s, far_r, fin_s, fin_r,
+    loc, kv_ss, kv_rs, q_ss, q_rs, s1_ss, s1_rs, x_ss, x_rs, y_ss, y_rs, d_ss, d_rs, o_ss, o_rs,
+    po_sem, ag_ss, ag_rs, fw_ss, fw_rs, h_ss, h_rs, dd_ss, dd_rs, near_ss, near_rs, far_ss, far_rs,
+    fin_ss, fin_rs,
 ):
     sp = lax.axis_index("sp")
     core = lax.axis_index("tp")
@@ -216,30 +222,17 @@
     half_rows = rows // 2
     width = x_ref.shape[1]
     kv_heads = kv_ref.shape[1] // LANES
-    plane = n // 4
-    group = 2 * plane
-    tokens = n * rows
     q_tokens = kv_heads * rows
     units = w_ref.shape[1] // 3
-    head_at = rem(sp, kv_heads)
-    q_base = sp - head_at
-    place = rem(sp, plane)
-    side = rem(sp // plane, 2)
-    wing = sp // (2 * plane)
-    member = wing * plane + place
-
-    def chip(m, at_side):
-        return (m // plane) * (2 * plane) + at_side * plane + rem(m, plane)
-
-    def ahead(d):
-        return rem(wing + d // plane, 2) * plane + rem(place + rem(d, plane), plane)
-
-    def behind(d):
-        return rem(wing + d // plane, 2) * plane + rem(
-            place + plane - rem(d, plane), plane
-        )
-
-    twin = chip(member, 1 - side)
+    place = rem(sp, PLANE)
+    z = sp // PLANE
+    q_base = sp - place
+    outer = jnp.logical_or(z == 0, z == PLANE - 1)
+    first_far = jnp.where(outer, 3, 2)
+    last_far = 5 - first_far
+
+    def chip(k, e):
+        return xor(z, k) * PLANE + xor(place, e)
 
     def remote(src, dst, ss, rs, device):
         return pltpu.make_async_remote_copy(
@@ -270,66 +263,117 @@
     pl.semaphore_wait(barrier, n)
 
     def q_copy(d):
-        t = q_base + rem(head_at + d, kv_heads)
+        t = q_base + rem(place + d, kv_heads)
         return remote(
-            q_ref.at[:, lane_block(t - q_base)], qbuf.at[span(head_at * rows, rows, rows)],
+            q_ref.at[:, lane_block(t - q_base)], qbuf.at[span(place * rows, rows, rows)],
             q_ss.at[d], q_rs.at[d], (t, core),
         )
 
-    def kv_copy(d):
-        t = rem(sp + d, n)
+    def kv_copy(k, e):
         return remote(
-            kv_ref.at[:, lane_block(rem(t, kv_heads))], kvbuf.at[span(sp * rows, rows, rows)],
-            kv_ss.at[d], kv_rs.at[d], (t, core),
-        )
-
-    up_part, down_part = slice(0, 2 * units), slice(2 * units, 3 * units)
-
-    def w_copy(d, part_at, ss, rs):
-        m = ahead(d)
+            kv_ref.at[:, lane_block(xor(place, e))], kvbuf.at[span(sp * rows, rows, rows)],
+            kv_ss.at[k * PLANE + e], kv_rs.at[k * PLANE + e], (chip(k, e), core),
+        )
+
+    def kv_relay(e):
+        at = kvbuf.at[span(chip(2, e) * rows, rows, rows)]
         return remote(
-            w_ref.at[m, part_at], wrecv.at[part_at, lane_block(sp)],
-            ss.at[d], rs.at[d], (chip(m, side), core),
-        )
-
-    def twin_first(part_at, ss, rs):
+            at, at, kv_ss.at[3 * PLANE + e], kv_rs.at[3 * PLANE + e], (chip(1, 0), core)
+        )
+
+    half = units // 2
+    pieces = (
+        slice(0, units), slice(units, 2 * units),
+        slice(2 * units, 2 * units + half), slice(2 * units + half, 3 * units),
+    )
+    ups, downs = (0, 1), (2, 3)
+
+    def block_of(j, source):
+        return wrecv.at[pieces[j], lane_block(source)]
+
+    def by_z(k, j):
+        i = j * PLANE + k
         return remote(
-            w_ref.at[member, part_at], wrecv.at[part_at, lane_block(sp)],
-            ss.at[0], rs.at[0], (twin, core),
-        )
-
-    def twin_copy(d, part_at, ss, rs):
-        at = wrecv.at[part_at, lane_block(chip(behind(d), side))]
-        return remote(at, at, ss.at[d], rs.at[d], (twin, core))
-
-    def pass_on(d, part_at, ss, rs, next_ss, next_rs):
-        dst = wrecv.at[part_at, lane_block(chip(behind(d), side))]
-        remote(dst, dst, ss.at[d], rs.at[d], (twin, core)).wait_recv()
-        twin_copy(d, part_at, next_ss, next_rs).start()
-
-    def twin_wait(d, part_at, ss, rs):
-        dst = wrecv.at[part_at, lane_block(chip(behind(d), 1 - side))]
-        remote(dst, dst, ss.at[d], rs.at[d], (twin, core)).wait_recv()
-
-    later = plane + plane // 2
-    gate_sems, gate_next = (w_ss, w_rs), (wf_ss, wf_rs)
-    down_sems, down_next = (dw_ss, dw_rs), (df_ss, df_rs)
+            w_ref.at[xor(z, k), pieces[j]], block_of(j, sp), s1_ss.at[i], s1_rs.at[i],
+            (chip(k, 0), core),
+        )
+
+    def across(k, j, e, ss, rs):
+        i = j * PLANE + k
+        src = w_ref.at[z, pieces[j]] if isinstance(k, int) and k == 0 else block_of(j, chip(k, 0))
+        return remote(src, block_of(j, chip(k, 0)), ss.at[i], rs.at[i], (chip(0, e), core))
+
+    def by_x(k, j):
+        return across(k, j, 1, x_ss, x_rs)
+
+    def by_y(k, j):
+        return across(k, j, 2, y_ss, y_rs)
+
+    def corner(k, j):
+        i = j * PLANE + k
+        from_x = j % 2 == 0
+        at = block_of(j, chip(k, 1 if from_x else 2))
+        return remote(at, at, d_ss.at[i], d_rs.at[i], (chip(0, 2 if from_x else 1), core))
+
+    def landed(j, source, k, ss, rs):
+        i = j * PLANE + k
+        at = block_of(j, source)
+        remote(at, at, ss.at[i], rs.at[i], (sp, mate)).wait_recv()
+
+    def spread(k, js):
+        for j in js:
+            by_x(k, j).start()
+        for j in js[::-1]:
+            by_y(k, j).start()
+
+    def take_z(k, js):
+        for j in js:
+            landed(j, chip(k, 0), k, s1_ss, s1_rs)
+        spread(k, js)
+
+    def take_corner(k, js):
+        landed(js[0], chip(k, 1), k, x_ss, x_rs)
+        corner(k, js[0]).start()
+        landed(js[1], chip(k, 2), k, y_ss, y_rs)
+        corner(k, js[1]).start()
+
+    def take_rest(k, js):
+        landed(js[1], chip(k, 1), k, x_ss, x_rs)
+        landed(js[0], chip(k, 2), k, y_ss, y_rs)
+        for j in js:
+            landed(j, chip(k, 3), k, d_ss, d_rs)
 
     own_q = pltpu.make_async_copy(
-        q_ref.at[:, lane_block(head_at)], qbuf.at[span(head_at * rows, rows, rows)], loc.at[0]
+        q_ref.at[:, lane_block(place)], qbuf.at[span(place * rows, rows, rows)], loc.at[0]
     )
     own_kv = pltpu.make_async_copy(
-        kv_ref.at[:, lane_block(head_at)], kvbuf.at[span(sp * rows, rows, rows)], loc.at[1]
-    )
-    own_w = pltpu.make_async_copy(w_ref.at[member], wrecv.at[:, lane_block(sp)], loc.at[2])
+        kv_ref.at[:, lane_block(place)], kvbuf.at[span(sp * rows, rows, rows)], loc.at[1]
+    )
+    own_w = pltpu.make_async_copy(w_ref.at[z], wrecv.at[:, lane_block(sp)], loc.at[2])
+    wo_copy = pltpu.make_async_copy(wo_ref, wo_buf, loc.at[3])
+
+    def far_up():
+        for k in (3, 2):
+            for j in ups:
+                by_z(k, j).start()
+
+    def far_down():
+        for k in (3, 2):
+            for j in downs:
+                by_z(k, j).start()
+
     own_q.start()
-    wo_copy = pltpu.make_async_copy(wo_ref, wo_buf, loc.at[3])
+    loop(1, kv_heads, lambda d: q_copy(d).start())
+    for k in (2, 1, 0):
+        for e in range(PLANE):
+            if k or e:
+                kv_copy(k, e).start()
     wo_copy.start()
+    for j in ups:
+        by_z(1, j).start()
+    pl.when(jnp.logical_not(outer))(far_up)
+    spread(0, ups)
     own_kv.start()
-    loop(1, kv_heads, lambda d: q_copy(d).start())
-    loop(1, n, lambda d: kv_copy(d).start())
-    loop(1, plane, lambda d: w_copy(d, up_part, *gate_sems).start())
-    loop(1, plane, lambda d: w_copy(d, down_part, *down_sems).start())
     own_w.start()
 
     lane = lax.broadcasted_iota(jnp.int32, (GRID_ROW_WIDTH, LANES), 1)
@@ -371,22 +415,23 @@
         qcat[later, :] = jnp.where(low, pltpu.roll(top, HEAD_SIZE, 1), rest).astype(BF)
 
     own_q.wait()
+    steps = rows // GRID_ROW_WIDTH
 
     def q_take(d):
-        s = rem(head_at + kv_heads - d, kv_heads)
+        s = rem(place + kv_heads - d, kv_heads)
         dst = qbuf.at[span(s * rows, rows, rows)]
 
         @pl.when(d > 0)
         def _():
             remote(dst, dst, q_ss.at[d], q_rs.at[d], (q_base + s, core)).wait_recv()
 
-        for r in range(rows // GRID_ROW_WIDTH):
-            make_q(s * (rows // GRID_ROW_WIDTH) + r)
+        for r in range(steps):
+            make_q(s * steps + r)
 
     loop(0, kv_heads, q_take)
-    twin_first(up_part, *gate_next).start()
-    loop(plane, later, lambda d: w_copy(d, up_part, *gate_sems).start())
-    steps = rows // GRID_ROW_WIDTH
+    pl.when(outer)(far_up)
+    for j in downs:
+        by_z(1, j).start()
 
     def make_k(r):
         at = span(r * GRID_ROW_WIDTH, GRID_ROW_WIDTH, GRID_ROW_WIDTH)
@@ -401,24 +446,27 @@
 
     own_kv.wait()
 
-    def kv_take(d):
-        s = rem(sp + n - d, n)
+    def kv_take(i):
+        s = chip(i // PLANE, rem(i, PLANE))
         dst = kvbuf.at[span(s * rows, rows, rows)]
 
-        @pl.when(d > 0)
+        @pl.when(i > 0)
         def _():
-            remote(dst, dst, kv_ss.at[d], kv_rs.at[d], (s, core)).wait_recv()
+            remote(dst, dst, kv_ss.at[i], kv_rs.at[i], (s, core)).wait_recv()
+
+        @pl.when(i // PLANE == 2)
+        def _():
+            kv_relay(rem(i, PLANE)).start()
 
         for r in range(steps):
             make_k(s * steps + r)
 
     loop(0, n, kv_take)
-    loop(1, plane, lambda d: pass_on(d, up_part, *gate_sems, *gate_next))
 
     def o_copy(d):
-        k = rem(head_at + d, kv_heads)
+        k = rem(place + d, kv_heads)
         return remote(
-            att_s.at[span(k * rows, rows, rows)], attbuf.at[:, lane_block(head_at)],
+            att_s.at[span(k * rows, rows, rows)], attbuf.at[:, lane_block(place)],
             o_ss.at[d], o_rs.at[d], (q_base + k, core),
         )
 
@@ -438,18 +486,23 @@
         ).astype(BF)
 
     def attend_send(d):
-        k = rem(head_at + d, kv_heads)
+        k = rem(place + d, kv_heads)
         att_s[span(k * rows, rows, rows), :] = attend(k)
 
         @pl.when(d < kv_heads)
         def _():
             o_copy(d).start()
 
+        @pl.when(d == 2)
+        def _():
+            take_corner(0, ups)
+
     loop(1, kv_heads + 1, attend_send)
-    attbuf[:, lane_block(head_at)] = att_s[span(head_at * rows, rows, rows), :]
+    attbuf[:, lane_block(place)] = att_s[span(place * rows, rows, rows), :]
+    take_z(1, ups)
 
     def o_wait(d):
-        s = rem(head_at + kv_heads - d, kv_heads)
+        s = rem(place + kv_heads - d, kv_heads)
         dst = attbuf.at[:, lane_block(s)]
         remote(dst, dst, o_ss.at[d], o_rs.at[d], (q_base + s, core)).wait_recv()
 
@@ -471,220 +524,213 @@
     normed = (middle * scaled * fg_ref[...]).astype(BF)
 
     def slot(k, c):
-        return allnorm.at[span(k * rows + c * half_rows, half_rows, half_rows)]
-
-    allnorm[span(member * rows + core * half_rows, half_rows, half_rows), :] = normed
-
-    def ag_copy(d):
-        to = ahead(rem(d, plane)) if d != plane else ahead(d)
-        of = member if d <= plane else (1 - wing) * plane + place
-        return remote(
-            slot(of, core), slot(of, core), ag_ss.at[d], ag_rs.at[d], (chip(to, side), core)
-        )
-
-    def fw_copy(d):
-        s = behind(d)
-        return remote(slot(s, core), slot(s, core), fw_ss.at[d], fw_rs.at[d], (sp, mate))
-
-    def ag_wait(d):
-        s = behind(d)
-        remote(slot(s, core), slot(s, core), ag_ss.at[d], ag_rs.at[d], (sp, mate)).wait_recv()
-        fw_copy(d).start()
-
-    ag_copy(plane).start()
-    for d in range(1, plane):
-        ag_copy(d).start()
+        return allnorm.at[span(xor(z, k) * rows + c * half_rows, half_rows, half_rows)]
+
+    allnorm[span(z * rows + core * half_rows, half_rows, half_rows), :] = normed
+
+    def ag_copy(k):
+        at = slot(2 if k == 3 else 0, core)
+        return remote(at, at, ag_ss.at[k], ag_rs.at[k], (chip(1 if k == 3 else k, 0), core))
+
+    def fw_copy(k):
+        at = slot(k, core)
+        return remote(at, at, fw_ss.at[k], fw_rs.at[k], (sp, mate))
+
+    def ag_take(k):
+        at = slot(k, core)
+        remote(at, at, ag_ss.at[k], ag_rs.at[k], (sp, mate)).wait_recv()
+        if k == 2:
+            ag_copy(3).start()
+        fw_copy(k).start()
+
+    ag_copy(2).start()
+    ag_copy(1).start()
     fw_copy(0).start()
-
+    pl.when(jnp.logical_not(outer))(far_down)
+    take_corner(1, ups)
+    spread(0, downs)
+    take_z(first_far, ups)
+    take_corner(0, downs)
+    take_z(1, downs)
+    ag_take(1)
+    take_z(last_far, ups)
+    take_corner(first_far, ups)
+    ag_take(2)
+    take_corner(1, downs)
+    take_corner(last_far, ups)
+    ag_take(3)
+    pl.when(outer)(far_down)
     own_w.wait()
-    loop(later, group, lambda d: w_copy(d, up_part, *gate_sems).start())
-    twin_first(down_part, *down_next).start()
-    loop(1, plane, lambda d: pass_on(d, down_part, *down_sems, *down_next))
-    loop(plane, later, lambda d: pass_on(d, up_part, *gate_sems, *gate_next))
-    ag_wait(plane)
-    for d in range(plane + 1, group):
-        ag_copy(d).start()
-    loop(plane, group, lambda d: w_copy(d, down_part, *down_sems).start())
-    loop(later, group, lambda d: pass_on(d, up_part, *gate_sems, *gate_next))
-
-    def up(block):
-        both = nt(block, wrecv[: 2 * units, :]).astype(BF).astype(F32)
-        return both[:, :units], both[:, units:]
-
-    seg = plane * rows
-    pitch = seg + 16
-
-    def row_of(m):
-        return (m // plane) * pitch + rem(m, plane) * rows
-
-    def take(d):
-        @pl.when(jnp.logical_and(d > 0, d != plane))
-        def _():
-            ag_wait(d)
-
-    def mate_wait(d):
-        s = behind(d)
-        remote(slot(s, mate), slot(s, mate), fw_ss.at[d], fw_rs.at[d], (sp, mate)).wait_recv()
-
-    def up_rows(k):
-        side_at = rem(wing + k, 2)
-        loop(k * plane, (k + 1) * plane, mate_wait)
-        gate, value = up(allnorm[span(side_at * seg, seg, rows), :])
-        at = span(side_at * pitch + 8, seg, 8)
-        pre_g[at, :] = gate
-        pre_v[at, :] = value
-
-    loop(0, group, take)
-    loop(0, group, lambda d: twin_wait(d, up_part, *gate_next))
-    loop(plane, group, lambda d: pass_on(d, down_part, *down_sems, *down_next))
-    loop(0, 2, up_rows)
-
-    edge_at = (8, 8 + seg - 1, pitch + 8, pitch + 8 + seg - 1)
+    for k in range(PLANE):
+        at = slot(k, mate)
+        remote(at, at, fw_ss.at[k], fw_rs.at[k], (sp, mate)).wait_recv()
+    for k in (0, 1, first_far, last_far):
+        take_rest(k, ups)
+
+    pitch = rows + 16
+    for pre, j in ((pre_g, 0), (pre_v, 1)):
+        both = nt(allnorm[...], wrecv[pieces[j], :]).astype(BF).astype(F32)
+        for k in range(PLANE):
+            pre[k * pitch + 8 : k * pitch + 8 + rows, :] = both[k * rows : (k + 1) * rows]
+
     edge_s[...] = jnp.concatenate(
         [
-            jnp.concatenate([pre[k : k + 1, :] for k in edge_at] * 2, axis=0)
+            pre[k * pitch + at : k * pitch + at + 1, :]
+            for at in (8, 8 + rows - 1)
             for pre in (pre_g, pre_v)
+            for k in range(PLANE)
         ],
         axis=0,
     )
-    edge_copy = remote(edge_s, edge_r, h_sem.at[0], h_sem.at[1], (twin, core))
-    edge_copy.start()
-    loop(0, group, lambda d: twin_wait(d, down_part, *down_next))
-    edge_copy.wait_recv()
-    for pre, first_row in ((pre_g, 0), (pre_v, 8)):
-        near = [
-            jnp.broadcast_to(edge_r[first_row + k : first_row + k + 1, :], (8, units))
-            for k in range(4)
+
+    def edge_copy(h):
+        at = slice(8 * h, 8 * h + 8)
+        to = q_base + rem(place + (PLANE - 1, 1)[h], PLANE)
+        return remote(edge_s.at[at], edge_r.at[at], h_ss.at[h], h_rs.at[h], (to, core))
+
+    edge_copy(0).start()
+    edge_copy(1).start()
+    take_z(first_far, downs)
+    edge_copy(0).wait_recv()
+    edge_copy(1).wait_recv()
+    none = jnp.zeros((8, units), F32)
+    for pre, at in ((pre_g, 0), (pre_v, PLANE)):
+        after = [jnp.broadcast_to(edge_r[at + k : at + k + 1, :], (8, units)) for k in range(PLANE)]
+        ahead = [
+            jnp.broadcast_to(edge_r[8 + at + k : 8 + at + k + 1, :], (8, units))
+            for k in range(PLANE)
         ]
-        none = jnp.zeros((8, units), F32)
-        pre[0:8, :] = jnp.where(side == 0, none, near[1])
-        pre[8 + seg : pitch, :] = jnp.where(side == 0, near[0], near[2])
-        pre[pitch : pitch + 8, :] = jnp.where(side == 0, near[1], near[3])
-        pre[pitch + 8 + seg :, :] = jnp.where(side == 0, near[2], none)
+        for k in range(PLANE):
+            here = k * pitch
+            pre[here : here + 8, :] = jnp.where(
+                place == 0, ahead[k - 1] if k else none, ahead[k]
+            )
+            pre[here + 8 + rows : here + pitch, :] = jnp.where(
+                place == PLANE - 1, after[k + 1] if k + 1 < PLANE else none, after[k]
+            )
 
     def convolve(ref, taps, k):
-        block = ref[span(row_of(k), rows + 16, 8), :]
+        block = ref[span(k * pitch, rows + 16, 8), :]
         return (
             taps[0:1, :] * block[7 : 7 + rows]
             + taps[1:2, :] * block[8 : 8 + rows]
             + taps[2:3, :] * block[9 : 9 + rows]
         )
 
-    def dd_copy(d):
-        return remote(
-            part.at[d, span(mate * half_rows, half_rows, half_rows)], ddbuf.at[d],
-            dd_ss.at[d], dd_rs.at[d], (sp, mate),
-        )
-
-    def c_copy(d, to):
-        return remote(rs_s.at[d], rs_r.at[d], c_ss.at[d], c_rs.at[d], (chip(to, side), core))
-
-    def c_near(d):
-        return c_copy(d, ahead(rem(d, plane)))
-
-    quarter_rows = half_rows // 2
-
-    def c_half(d, h, to):
-        at = span(h * quarter_rows, quarter_rows, quarter_rows)
-        return remote(
-            rs_s.at[d, at], rs_r.at[d, at], ch_ss.at[2 * d + h], ch_rs.at[2 * d + h],
-            (chip(to, side), core),
-        )
-
-    def c_cross(d, h):
-        return c_half(d, h, ahead(rem(d, plane)))
-
-    def combine(d):
-        dd_copy(d).wait_recv()
-        return part[d, mine, :].astype(F32) + ddbuf[d].astype(F32)
-
-    def send_sum(d):
-        rs_s[d] = combine(d).astype(BF)
-
-        @pl.when(d < plane)
-        def _():
-            c_near(d).start()
-
-        @pl.when(d > plane)
-        def _():
-            c_cross(d, 0).start()
-
-    def order(j):
-        return plane * (1 - j // plane) + rem(j + 1, plane)
-
-    def down(j):
-        d = order(j)
-        k = ahead(d)
+    quad = PLANE * half_rows
+
+    def gated(k):
         gate = convolve(pre_g, cg_ref, k)
         value = convolve(pre_v, cv_ref, k)
         hidden = (gate / (1.0 + jnp.exp(-gate)) * value).astype(BF)
-        part[d] = jnp.dot(hidden, wrecv[2 * units :, :], preferred_element_type=F32).astype(BF)
-        dd_copy(d).start()
-        last = order(jnp.maximum(j - 1, 0))
-
-        @pl.when(jnp.logical_and(j > 0, rem(last, plane) > 0))
-        def _():
-            send_sum(last)
-
-        @pl.when(j == plane)
-        def _():
-            loop(plane + 1, group, lambda k: c_cross(k, 1).start())
-
-    loop(0, group, down)
-
-    def add_in(d):
-        remote(rs_r.at[d], rs_r.at[d], c_ss.at[d], c_rs.at[d], (sp, mate)).wait_recv()
-        own_sum[...] = own_sum[...] + rs_r[d].astype(F32)
-
-    own_sum[...] = combine(plane)
-    far = (1 - wing) * plane + place
-
-    def far_send(h):
-        at = span(h * quarter_rows, quarter_rows, quarter_rows)
-
-        def half_in(d):
-            c_cross(d, h).wait_recv()
-            own_sum[at, :] = own_sum[at, :] + rs_r[d, at, :].astype(F32)
-
-        loop(plane + 1, group, half_in)
-        rs_s[plane, at, :] = own_sum[at, :].astype(BF)
-        c_half(plane, h, far).start()
-
-    loop(0, 2, far_send)
-    own_sum[...] = mid[...] + combine(0)
-    loop(1, plane, add_in)
-
-    def far_take(h):
-        at = span(h * quarter_rows, quarter_rows, quarter_rows)
-        c_half(plane, h, far).wait_recv()
-        own_sum[at, :] = own_sum[at, :] + rs_r[plane, at, :].astype(F32)
-
-    loop(0, 2, far_take)
-    fin_s[...] = own_sum[...].astype(BF)
-    fin_copy = remote(fin_s, fin_r, fin_sem.at[0], fin_sem.at[1], (sp, mate))
-    fin_copy.start()
-    out_ref[mine, :] = fin_s[...]
+        for c in range(2):
+            hid[span(c * quad + k * half_rows, half_rows, half_rows), :] = hidden[
+                c * half_rows : (c + 1) * half_rows
+            ]
+
+    loop(0, PLANE, gated)
+    chunk = PLANE * LANES
+
+    def columns(c):
+        return slice(c * chunk, (c + 1) * chunk)
+
+    def dd_copy(c):
+        return remote(
+            part.at[c, span(mate * quad, quad, quad)], ddbuf.at[c], dd_ss.at[c], dd_rs.at[c],
+            (sp, mate),
+        )
+
+    def near_copy(c):
+        return remote(near_s.at[c], near_r.at[c], near_ss.at[c], near_rs.at[c], (chip(1, 0), core))
+
+    def far_copy(c):
+        return remote(far_s.at[c], far_r.at[c], far_ss.at[c], far_rs.at[c], (chip(2, 0), core))
+
+    def fin_copy(c):
+        return remote(
+            fin_s.at[:, columns(c)], fin_r.at[:, columns(c)], fin_ss.at[c], fin_rs.at[c], (sp, mate)
+        )
+
+    def summed_for(c, k):
+        at = xor(z, k) * half_rows
+        return (
+            part[c, span(core * quad + at, half_rows, half_rows), :].astype(F32)
+            + ddbuf[c, span(at, half_rows, half_rows), :].astype(F32)
+        )
+
+    def down(c):
+        take_rest(xor(z, c), downs)
+        part[c] = jnp.dot(
+            hid[...], wrecv[2 * units :, columns(c)], preferred_element_type=F32
+        ).astype(BF)
+        dd_copy(c).start()
+
+    def to_near(c):
+        dd_copy(c).wait_recv()
+        near_s[c, :half_rows, :] = summed_for(c, 1).astype(BF)
+        near_s[c, half_rows:, :] = summed_for(c, 3).astype(BF)
+        near_copy(c).start()
+
+    def to_far(c):
+        near_copy(c).wait_recv()
+        far_s[c] = (summed_for(c, 2) + near_r[c, half_rows:, :].astype(F32)).astype(BF)
+        far_copy(c).start()
+
+    def finish(c):
+        ours = mid[:, columns(c)] + summed_for(c, 0) + near_r[c, :half_rows, :].astype(F32)
+        far_copy(c).wait_recv()
+        fin_s[:, columns(c)] = (ours + far_r[c].astype(F32)).astype(BF)
+        fin_copy(c).start()
+        out_ref[mine, columns(c)] = fin_s[:, columns(c)]
+
+    take_corner(first_far, downs)
+    take_z(last_far, downs)
+    down(0)
+    down(3)
+    to_near(0)
+    take_corner(last_far, downs)
+    to_near(3)
+    down(1)
+    to_far(0)
+    to_near(1)
+    down(2)
+    to_far(3)
+    to_near(2)
+    to_far(1)
+    finish(0)
+    finish(3)
+    to_far(2)
+    finish(1)
+    finish(2)
 
     loop(1, kv_heads, lambda d: q_copy(d).wait_send())
-    loop(1, n, lambda d: kv_copy(d).wait_send())
-    loop(1, group, lambda d: w_copy(d, up_part, *gate_sems).wait_send())
-    loop(1, group, lambda d: w_copy(d, down_part, *down_sems).wait_send())
-    loop(0, group, lambda d: twin_copy(d, up_part, *gate_next).wait_send())
-    loop(0, group, lambda d: twin_copy(d, down_part, *down_next).wait_send())
+    for k in (2, 1, 0):
+        for e in range(PLANE):
+            if k or e:
+                kv_copy(k, e).wait_send()
+    for e in range(PLANE):
+        kv_relay(e).wait_send()
+    for j in ups + downs:
+        for k in range(PLANE):
+            if k:
+                by_z(k, j).wait_send()
+            by_x(k, j).wait_send()
+            by_y(k, j).wait_send()
+            corner(k, j).wait_send()
     loop(1, kv_heads, lambda d: o_copy(d).wait_send())
     po_copy.wait_send()
-    for d in range(1, group):
-        ag_copy(d).wait_send()
-    loop(0, group, lambda d: fw_copy(d).wait_send())
-    edge_copy.wait_send()
-    loop(0, group, lambda d: dd_copy(d).wait_send())
-    loop(1, plane, lambda d: c_near(d).wait_send())
+    for k in range(PLANE):
+        if k:
+            ag_copy(k).wait_send()
+        fw_copy(k).wait_send()
     for h in range(2):
-        for d in range(plane + 1, group):
-            c_cross(d, h).wait_send()
-        c_half(plane, h, far).wait_send()
-    fin_copy.wait_send()
-    fin_copy.wait_recv()
+        edge_copy(h).wait_send()
+    for c in range(PLANE):
+        dd_copy(c).wait_send()
+        near_copy(c).wait_send()
+        far_copy(c).wait_send()
+        fin_copy(c).wait_send()
+        fin_copy(c).wait_recv()
     out_ref[span(mate * half_rows, half_rows, half_rows), :] = fin_r[...]
 
 
@@ -704,41 +750,39 @@
 ):
     rows, width = x_rows.shape
     kv_heads = keys.shape[1] // HEAD_SIZE
-    plane = n // 4
-    group = 2 * plane
-    unit_local = gate_weight.shape[1]
-    units = unit_local // group
+    units = gate_weight.shape[1] // PLANE
     depth = gate_weight.shape[0]
     kv = jnp.concatenate(
         [keys.reshape(rows, kv_heads, HEAD_SIZE), values.reshape(rows, kv_heads, HEAD_SIZE)], axis=-1
     ).reshape(rows, kv_heads * LANES)
     turned = [
-        w.T.reshape(group, units, depth) for w in (gate_weight, value_weight, down_weight)
+        w.T.reshape(PLANE, units, depth) for w in (gate_weight, value_weight, down_weight)
     ]
     weights = jnp.concatenate(turned, axis=1)
-    at = lax.axis_index("sp")
-    chip = (at // group) * plane + rem(at, plane)
-    taps = [lax.dynamic_slice_in_dim(t, chip * units, units, 1) for t in (conv_gate, conv_value)]
+    at = lax.axis_index("sp") // PLANE
+    taps = [lax.dynamic_slice_in_dim(t, at * units, units, 1) for t in (conv_gate, conv_value)]
     cos, sin = rotary_tables(max(GRID_ROW_WIDTH, n * rows // GRID_ROW_WIDTH))
-    tokens, q_tokens, span_rows = n * rows, kv_heads * rows, group * rows
+    tokens, q_tokens, span_rows = n * rows, kv_heads * rows, PLANE * rows
     half_rows = rows // 2
+    chunk = PLANE * LANES
     dma = pltpu.SemaphoreType.DMA
     vm = pltpu.VMEM
+    padded = span_rows + 16 * PLANE
     scratch = [
         vm(out_weight.shape, BF), vm((tokens, LANES), BF), vm((q_tokens, LANES), BF), vm((tokens, 2 * LANES), BF),
         vm((2 * q_tokens, LANES), BF), vm((q_tokens, LANES), BF), vm((rows, kv_heads * LANES), BF),
         vm((rows, width), BF), vm((half_rows, width), BF), vm((half_rows, width), F32),
         vm((span_rows, width), BF), vm((16, units), F32),
         vm((16, units), F32), vm((3 * units, width), BF),
-        vm((span_rows + 32, units), F32), vm((span_rows + 32, units), F32),
-        vm((group, rows, width), BF), vm((group, half_rows, width), BF),
-        vm((half_rows, width), F32), vm((group, half_rows, width), BF),
-        vm((group, half_rows, width), BF), vm((half_rows, width), BF), vm((half_rows, width), BF),
-        dma((4,)), dma((n,)), dma((n,)), dma((kv_heads,)), dma((kv_heads,)), *[dma((group,))] * 8,
-        dma((kv_heads,)), dma((kv_heads,)), dma((2,)), dma((group,)), dma((group,)),
-        dma((group,)), dma((group,)), dma((2 * group,)), dma((2 * group,)), dma((2,)),
-        dma((group,)), dma((group,)),
-        dma((group,)), dma((group,)), dma((2,)),
+        vm((padded, units), F32), vm((padded, units), F32), vm((span_rows, units), BF),
+        vm((PLANE, span_rows, chunk), BF), vm((PLANE, span_rows // 2, chunk), BF),
+        vm((PLANE, rows, chunk), BF), vm((PLANE, rows, chunk), BF),
+        vm((PLANE, half_rows, chunk), BF), vm((PLANE, half_rows, chunk), BF),
+        vm((half_rows, width), BF), vm((half_rows, width), BF),
+        dma((4,)), dma((n,)), dma((n,)), dma((kv_heads,)), dma((kv_heads,)),
+        *[dma((4 * PLANE,))] * 8,
+        dma((kv_heads,)), dma((kv_heads,)), dma((2,)),
+        *[dma((PLANE,))] * 4, dma((2,)), dma((2,)), *[dma((PLANE,))] * 8,
     ]
     args = (
         x_rows, queries, kv, query_norm_gain[None, :], key_norm_gain[None, :],
@@ -762,19 +806,19 @@
 def suits(mesh, sizes):
     n, pair = mesh.shape["sp"], mesh.shape["tp"]
     x_rows, queries, keys, gate = sizes
-    if pair != 2 or n % 4:
+    if pair != 2 or n != PLANE * PLANE:
         return False
-    rows, group = x_rows[0] // n, n // 2
+    rows = x_rows[0] // n
     heads = keys[1] // pair // HEAD_SIZE
     units = gate[1] // pair
     return (
         rows % GRID_ROW_WIDTH == 0
         and rows % 32 == 0
         and queries[1] == 2 * keys[1]
-        and n % heads == 0
+        and heads == PLANE
         and 2 * HEAD_SIZE == LANES
         and x_rows[1] == n * LANES
-        and units % (16 * group) == 0
+        and units % (LANES * PLANE) == 0
     )
 
 

time: 130 us -> 143 us (1.10)
  Pallas kernels: 120 us -> 133 us
    pallas_call x1, Pallas kernels: 120 us -> 133 us  [kernel_shards(): pl.pallas_call(lambda *refs: layer_kernel(n, *refs), out_shape=jax.ShapeD...]
where the time goes in v1:
time: 143 us
  Pallas kernels  133 us (93%)
  local copies, waits for them, and re-layouts  7.41 us (5%)
  other arithmetic  2.22 us (2%)
    pallas_call x1, Pallas kernels, kernel_shards(): pl.pallas_call(lambda *refs: layer_kernel(n, *refs), out_shape=jax.ShapeD...  133 us
    transpose x3, local copies, waits for them, and re-layouts, kernel_shards(): w.T.reshape(PLANE, units, depth)  3.14 us

profile of v1, /device:TPU:0, one launch (start us, length us, event | category | flops | bytes accessed | tf_op | source)
XLA Modules:
  0.0 142.8 jit_solution(824582290718048944)
XLA Ops:
  0.0 0.0 copy-start
  0.0 1.4 constant_dynamic-slice_fusion
  1.4 0.8 sine_multiply_fusion
  2.2 1.4 copy.22
  3.6 1.4 copy.20
  5.0 0.0 copy-done
  5.0 0.3 copy.21
  5.3 0.0 copy-start.1
  5.3 0.0 copy-start.2
  5.4 1.4 %pad_maximum_fusion.refs_9_ = bf16[4,1920,128]{2,1,0:T(8,128)(2,1)} fusion(bf16[4,640,128]{2,1,0:T(8,128)(2,1)S(1)} %bitcast.12, bf16[4,640,128]{2,1,0:T(8,128)(2,1)S(1)} %bitcast.14, bf16[4,640,128]{2,1,0:T(8,128)(2,1)S(1)} %bitcast.13), kind=kLoop, calls=%fused_computation | loop fusion | flops 5898240 | bytes 3932160 | tf_op jit(solution)/shard_map/concatenate | solution.py:761
  6.8 0.0 copy-done.1
  6.8 0.1 copy.17
  6.9 0.0 copy-done.2
  6.9 0.1 copy.18
  7.1 0.8 copy.23.refs_2_
  7.8 133.1 %layer.1 = bf16[128,2048]{1,0:T(8,128)(2,1)} custom-call(bf16[128,2048]{1,0:T(8,128)(2,1)} %refs_0_.1, bf16[128,512]{1,0:T(8,128)(2,1)} %refs_1_.1, bf16[128,512]{1,0:T(8,128)(2,1)} %copy.23.refs_2_, f32[1,64]{1,0:T(1,128)} %bitcast.22, f32[1,64]{1,0:T(1,128)} %bitcast.23, f32[64,128]{1,0:T(8,128)} %get-tuple-element.6.refs_5_, ...), custom_call_target="tpu_custom_call" | custom-call | tf_op jit(solution)/shard_map/layer/pallas_call | solution.py:791
  140.9 1.9 %copy.25 = bf16[128,2048]{1,0:T(8,128)(2,1)} copy(bf16[128,2048]{1,0:T(8,128)(2,1)} %layer.1) | data formatting | bytes 1048576
  (2 shorter events, 0.0 us)
Async XLA Ops:
  0.0 5.0 %copy-start = (bf16[128,2560]{1,0:T(8,128)(2,1)S(1)}, bf16[128,2560]{1,0:T(8,128)(2,1)}, u32[]{:S(2)}) copy-start(bf16[128,2560]{1,0:T(8,128)(2,1)} %param.22) | copy-start | bytes 1966084
  5.3 1.5 %copy-start.1 = (bf16[128,256]{1,0:T(8,128)(2,1)S(1)}, bf16[128,256]{1,0:T(8,128)(2,1)}, u32[]{:S(2)}) copy-start(bf16[128,256]{1,0:T(8,128)(2,1)} %param.15) | copy-start | bytes 196612
  5.3 1.6 %copy-start.2 = (bf16[128,256]{1,0:T(8,128)(2,1)S(1)}, bf16[128,256]{1,0:T(8,128)(2,1)}, u32[]{:S(2)}) copy-start(bf16[128,256]{1,0:T(8,128)(2,1)} %param.16) | copy-start | bytes 196612

commit v2 on v1

--- a/solution.py
+++ b/solution.py
@@ -3,6 +3,7 @@
 
 import jax
 import jax.numpy as jnp
+import numpy as np
 from jax import lax
 from jax.experimental import pallas as pl
 from jax.experimental.pallas import tpu as pltpu
@@ -207,23 +208,24 @@
 
 
 def layer_kernel(
-    n, x_ref, q_ref, kv_ref, qg_ref, kg_ref, cos_ref, sin_ref, wo_ref, fg_ref, w_ref,
-    cg_ref, cv_ref, out_ref,
-    wo_buf, kvbuf, qbuf, kcat, qcat, att_s, attbuf, po_s, po_r, mid, allnorm, edge_s, edge_r, wrecv,
+    n, x_hbm, q_hbm, k_hbm, v_hbm, qg_hbm, kg_hbm, cos_hbm, sin_hbm, wo_ref, fg_hbm, gate_hbm,
+    value_hbm, down_hbm, cg_hbm, cv_hbm, out_ref,
+    x_ref, k_ref, v_ref, kv_ref, qg_ref, kg_ref, cos_ref, sin_ref, fg_ref, cg_ref, cv_ref,
+    wo_buf, kvbuf, qbuf, kcat, qcat, att_s, attbuf, po_s, po_r, mid, allnorm, edge_s, w_gate, w_value, w_down,
     pre_g, pre_v, hid, part, ddbuf, near_s, near_r, far_s, far_r, fin_s, fin_r,
-    loc, kv_ss, kv_rs, q_ss, q_rs, s1_ss, s1_rs, x_ss, x_rs, y_ss, y_rs, d_ss, d_rs, o_ss, o_rs,
+    loc, kv_ss, kf_ss, kv_rs, q_ss, q_rs, s1_ss, s1_rs, x_ss, x_rs, y_ss, y_rs, d_ss, d_rs, o_ss, o_rs,
     po_sem, ag_ss, ag_rs, fw_ss, fw_rs, h_ss, h_rs, dd_ss, dd_rs, near_ss, near_rs, far_ss, far_rs,
     fin_ss, fin_rs,
 ):
     sp = lax.axis_index("sp")
     core = lax.axis_index("tp")
     mate = 1 - core
-    rows = x_ref.shape[0]
+    rows, width = x_hbm.shape
     half_rows = rows // 2
-    width = x_ref.shape[1]
     kv_heads = kv_ref.shape[1] // LANES
     q_tokens = kv_heads * rows
-    units = w_ref.shape[1] // 3
+    units = w_gate.shape[1]
+    depth = gate_hbm.shape[0]
     place = rem(sp, PLANE)
     z = sp // PLANE
     q_base = sp - place
@@ -252,6 +254,26 @@
 
         lax.fori_loop(lo, hi, step, 0)
 
+    mine = span(core * half_rows, half_rows, half_rows)
+    loads = [
+        pltpu.make_async_copy(src, dst, loc.at[4 + i])
+        for i, (src, dst) in enumerate(
+            (
+                (k_hbm, k_ref), (v_hbm, v_ref), (cos_hbm, cos_ref), (sin_hbm, sin_ref),
+                (qg_hbm, qg_ref), (kg_hbm, kg_ref), (fg_hbm, fg_ref), (cg_hbm, cg_ref),
+                (cv_hbm, cv_ref), (x_hbm.at[mine], x_ref),
+            )
+        )
+    ]
+    own_q = pltpu.make_async_copy(
+        q_hbm.at[:, lane_block(place)], qbuf.at[span(place * rows, rows, rows)], loc.at[0]
+    )
+    for load in loads[:2]:
+        load.start()
+    own_q.start()
+    for load in loads[2:]:
+        load.start()
+
     barrier = pltpu.get_barrier_semaphore()
 
     def greet(d):
@@ -260,47 +282,67 @@
 
     loop(1, n, greet)
     pl.semaphore_signal(barrier, inc=1, device_id=(sp, mate), device_id_type=MESH)
+    for load in loads[:2]:
+        load.wait()
+    whole_lane = lax.broadcasted_iota(jnp.int32, (rows, LANES), 1) < HEAD_SIZE
+    for b in range(kv_heads // 2):
+        at = slice(b * LANES, (b + 1) * LANES)
+        k_pair, v_pair = k_ref[:, at].astype(F32), v_ref[:, at].astype(F32)
+        kv_ref[:, 2 * b * LANES : (2 * b + 1) * LANES] = jnp.where(
+            whole_lane, k_pair, pltpu.roll(v_pair, HEAD_SIZE, 1)
+        ).astype(BF)
+        kv_ref[:, (2 * b + 1) * LANES : (2 * b + 2) * LANES] = jnp.where(
+            whole_lane, pltpu.roll(k_pair, HEAD_SIZE, 1), v_pair
+        ).astype(BF)
     pl.semaphore_wait(barrier, n)
 
     def q_copy(d):
         t = q_base + rem(place + d, kv_heads)
         return remote(
-            q_ref.at[:, lane_block(t - q_base)], qbuf.at[span(place * rows, rows, rows)],
+            q_hbm.at[:, lane_block(t - q_base)], qbuf.at[span(place * rows, rows, rows)],
             q_ss.at[d], q_rs.at[d], (t, core),
         )
 
-    def kv_copy(k, e):
+    across_far = jnp.where(outer, 2, 3)
+    inner = jnp.logical_not(outer)
+
+    def kv_copy(k, e, far=False):
+        sent, sent_at = (kf_ss, e) if far else (kv_ss, k * PLANE + e)
         return remote(
             kv_ref.at[:, lane_block(xor(place, e))], kvbuf.at[span(sp * rows, rows, rows)],
-            kv_ss.at[k * PLANE + e], kv_rs.at[k * PLANE + e], (chip(k, e), core),
-        )
-
-    def kv_relay(e):
-        at = kvbuf.at[span(chip(2, e) * rows, rows, rows)]
-        return remote(
-            at, at, kv_ss.at[3 * PLANE + e], kv_rs.at[3 * PLANE + e], (chip(1, 0), core)
-        )
-
-    half = units // 2
+            sent.at[sent_at], kv_rs.at[k * PLANE + e], (chip(k, e), core),
+        )
+
+    def kv_relay(k, e):
+        at = kvbuf.at[span(chip(k, e) * rows, rows, rows)]
+        i = (5 - k) * PLANE + e
+        return remote(at, at, kv_ss.at[i], kv_rs.at[i], (chip(1, 0), core))
+
+    half = depth // 2
     pieces = (
-        slice(0, units), slice(units, 2 * units),
-        slice(2 * units, 2 * units + half), slice(2 * units + half, 3 * units),
+        (gate_hbm, w_gate, 0, depth), (value_hbm, w_value, 0, depth),
+        (down_hbm, w_down, 0, half), (down_hbm, w_down, half, half),
     )
     ups, downs = (0, 1), (2, 3)
 
     def block_of(j, source):
-        return wrecv.at[pieces[j], lane_block(source)]
+        _, held, first_row, count = pieces[j]
+        return held.at[span(source * depth + first_row, count, count)]
+
+    def source_of(j, at_z):
+        given, _, first_row, count = pieces[j]
+        return given.at[first_row : first_row + count, span(at_z * units, units, LANES)]
 
     def by_z(k, j):
         i = j * PLANE + k
         return remote(
-            w_ref.at[xor(z, k), pieces[j]], block_of(j, sp), s1_ss.at[i], s1_rs.at[i],
+            source_of(j, xor(z, k)), block_of(j, sp), s1_ss.at[i], s1_rs.at[i],
             (chip(k, 0), core),
         )
 
     def across(k, j, e, ss, rs):
         i = j * PLANE + k
-        src = w_ref.at[z, pieces[j]] if isinstance(k, int) and k == 0 else block_of(j, chip(k, 0))
+        src = source_of(j, z) if isinstance(k, int) and k == 0 else block_of(j, chip(k, 0))
         return remote(src, block_of(j, chip(k, 0)), ss.at[i], rs.at[i], (chip(0, e), core))
 
     def by_x(k, j):
@@ -343,38 +385,53 @@
         for j in js:
             landed(j, chip(k, 3), k, d_ss, d_rs)
 
-    own_q = pltpu.make_async_copy(
-        q_ref.at[:, lane_block(place)], qbuf.at[span(place * rows, rows, rows)], loc.at[0]
-    )
     own_kv = pltpu.make_async_copy(
         kv_ref.at[:, lane_block(place)], kvbuf.at[span(sp * rows, rows, rows)], loc.at[1]
     )
-    own_w = pltpu.make_async_copy(w_ref.at[z], wrecv.at[:, lane_block(sp)], loc.at[2])
+    own_w = [
+        pltpu.make_async_copy(source_of(j, z), block_of(j, sp), loc.at[14 + j]) for j in ups + downs
+    ]
     wo_copy = pltpu.make_async_copy(wo_ref, wo_buf, loc.at[3])
 
-    def far_up():
-        for k in (3, 2):
-            for j in ups:
-                by_z(k, j).start()
+    def far_up(k):
+        for j in ups:
+            by_z(k, j).start()
 
     def far_down():
         for k in (3, 2):
             for j in downs:
                 by_z(k, j).start()
 
-    own_q.start()
     loop(1, kv_heads, lambda d: q_copy(d).start())
-    for k in (2, 1, 0):
+    for e in range(PLANE):
+        kv_copy(across_far, e, True).start()
+    for k in (1, 0):
         for e in range(PLANE):
             if k or e:
                 kv_copy(k, e).start()
     wo_copy.start()
-    for j in ups:
-        by_z(1, j).start()
-    pl.when(jnp.logical_not(outer))(far_up)
-    spread(0, ups)
+
+    def near_up():
+        for j in ups:
+            by_z(1, j).start()
+
+    def near_down():
+        for j in downs:
+            by_z(1, j).start()
+
+    pl.when(outer)(near_up)
+    far_up(across_far)
+
+    @pl.when(outer)
+    def _():
+        far_up(3)
+        near_down()
+
     own_kv.start()
-    own_w.start()
+    for copy in own_w:
+        copy.start()
+    for load in loads[2:]:
+        load.wait()
 
     lane = lax.broadcasted_iota(jnp.int32, (GRID_ROW_WIDTH, LANES), 1)
     low = lane < HEAD_SIZE
@@ -429,9 +486,6 @@
             make_q(s * steps + r)
 
     loop(0, kv_heads, q_take)
-    pl.when(outer)(far_up)
-    for j in downs:
-        by_z(1, j).start()
 
     def make_k(r):
         at = span(r * GRID_ROW_WIDTH, GRID_ROW_WIDTH, GRID_ROW_WIDTH)
@@ -447,16 +501,34 @@
     own_kv.wait()
 
     def kv_take(i):
-        s = chip(i // PLANE, rem(i, PLANE))
+        k = jnp.where(outer, i // PLANE, jnp.where(i < PLANE, 0, rem(i // PLANE, PLANE - 1) + 1))
+        e = rem(i, PLANE)
+        s = chip(k, e)
         dst = kvbuf.at[span(s * rows, rows, rows)]
 
         @pl.when(i > 0)
         def _():
-            remote(dst, dst, kv_ss.at[i], kv_rs.at[i], (s, core)).wait_recv()
-
-        @pl.when(i // PLANE == 2)
+            at = k * PLANE + e
+            remote(dst, dst, kv_ss.at[at], kv_rs.at[at], (s, core)).wait_recv()
+
+        @pl.when(jnp.logical_and(inner, k > 1))
         def _():
-            kv_relay(rem(i, PLANE)).start()
+            kv_relay(k, e).start()
+
+        @pl.when(jnp.logical_and(inner, i == 3 * PLANE - 1))
+        def _():
+            near_up()
+            far_up(2)
+            near_down()
+
+        @pl.when(jnp.logical_and(outer, i == 3 * PLANE))
+        def _():
+            take_corner(0, ups)
+
+        @pl.when(i == PLANE)
+        def _():
+            spread(0, ups)
+            spread(0, downs)
 
         for r in range(steps):
             make_k(s * steps + r)
@@ -487,19 +559,21 @@
 
     def attend_send(d):
         k = rem(place + d, kv_heads)
+
+        @pl.when(jnp.logical_and(inner, d == kv_heads))
+        def _():
+            take_corner(0, ups)
+            take_z(1, ups)
+            take_z(3, ups)
+
         att_s[span(k * rows, rows, rows), :] = attend(k)
 
         @pl.when(d < kv_heads)
         def _():
             o_copy(d).start()
 
-        @pl.when(d == 2)
-        def _():
-            take_corner(0, ups)
-
     loop(1, kv_heads + 1, attend_send)
     attbuf[:, lane_block(place)] = att_s[span(place * rows, rows, rows), :]
-    take_z(1, ups)
 
     def o_wait(d):
         s = rem(place + kv_heads - d, kv_heads)
@@ -515,8 +589,7 @@
         (sp, mate),
     )
     po_copy.start()
-    mine = span(core * half_rows, half_rows, half_rows)
-    base = x_ref[mine, :].astype(F32) + po_s[mine, :].astype(F32)
+    base = x_ref[...].astype(F32) + po_s[mine, :].astype(F32)
     po_copy.wait_recv()
     middle = base + po_r[...].astype(F32)
     mid[...] = middle
@@ -528,9 +601,13 @@
 
     allnorm[span(z * rows + core * half_rows, half_rows, half_rows), :] = normed
 
-    def ag_copy(k):
-        at = slot(2 if k == 3 else 0, core)
-        return remote(at, at, ag_ss.at[k], ag_rs.at[k], (chip(1 if k == 3 else k, 0), core))
+    def ag_copy(k, i):
+        at = slot(0, core)
+        return remote(at, at, ag_ss.at[i], ag_rs.at[k], (chip(k, 0), core))
+
+    def ag_relay(k):
+        at = slot(k, core)
+        return remote(at, at, ag_ss.at[5 - k], ag_rs.at[5 - k], (chip(1, 0), core))
 
     def fw_copy(k):
         at = slot(k, core)
@@ -539,46 +616,47 @@
     def ag_take(k):
         at = slot(k, core)
         remote(at, at, ag_ss.at[k], ag_rs.at[k], (sp, mate)).wait_recv()
-        if k == 2:
-            ag_copy(3).start()
+        if not isinstance(k, int):
+            pl.when(inner)(lambda: ag_relay(k).start())
         fw_copy(k).start()
 
-    ag_copy(2).start()
-    ag_copy(1).start()
+    ag_copy(across_far, 0).start()
+    ag_copy(1, 1).start()
     fw_copy(0).start()
-    pl.when(jnp.logical_not(outer))(far_down)
+    pl.when(inner)(far_down)
+    take_corner(0, downs)
+    pl.when(outer)(lambda: take_z(1, ups))
     take_corner(1, ups)
-    spread(0, downs)
-    take_z(first_far, ups)
-    take_corner(0, downs)
-    take_z(1, downs)
+    pl.when(outer)(lambda: take_z(3, ups))
+
+    @pl.when(inner)
+    def _():
+        take_z(2, ups)
+        take_corner(3, ups)
+        ag_take(first_far)
+        take_corner(2, ups)
+
+    @pl.when(outer)
+    def _():
+        take_z(2, ups)
+        take_corner(3, ups)
+        take_corner(2, ups)
+        far_down()
+        ag_take(first_far)
+
     ag_take(1)
-    take_z(last_far, ups)
-    take_corner(first_far, ups)
-    ag_take(2)
-    take_corner(1, downs)
-    take_corner(last_far, ups)
-    ag_take(3)
-    pl.when(outer)(far_down)
-    own_w.wait()
+    ag_take(last_far)
+    for copy in own_w:
+        copy.wait()
     for k in range(PLANE):
         at = slot(k, mate)
         remote(at, at, fw_ss.at[k], fw_rs.at[k], (sp, mate)).wait_recv()
-    for k in (0, 1, first_far, last_far):
-        take_rest(k, ups)
-
-    pitch = rows + 16
-    for pre, j in ((pre_g, 0), (pre_v, 1)):
-        both = nt(allnorm[...], wrecv[pieces[j], :]).astype(BF).astype(F32)
-        for k in range(PLANE):
-            pre[k * pitch + 8 : k * pitch + 8 + rows, :] = both[k * rows : (k + 1) * rows]
-
+    quad_rows = PLANE * rows
     edge_s[...] = jnp.concatenate(
         [
-            pre[k * pitch + at : k * pitch + at + 1, :]
-            for at in (8, 8 + rows - 1)
-            for pre in (pre_g, pre_v)
-            for k in range(PLANE)
+            allnorm[k * rows + at : k * rows + at + 1, :]
+            for at in (0, rows - 1)
+            for k in tuple(range(PLANE)) * (8 // PLANE)
         ],
         axis=0,
     )
@@ -586,21 +664,34 @@
     def edge_copy(h):
         at = slice(8 * h, 8 * h + 8)
         to = q_base + rem(place + (PLANE - 1, 1)[h], PLANE)
-        return remote(edge_s.at[at], edge_r.at[at], h_ss.at[h], h_rs.at[h], (to, core))
+        return remote(
+            edge_s.at[at], allnorm.at[quad_rows + 8 * h : quad_rows + 8 * h + 8],
+            h_ss.at[h], h_rs.at[h], (to, core),
+        )
 
     edge_copy(0).start()
     edge_copy(1).start()
-    take_z(first_far, downs)
+    take_z(1, downs)
+    take_z(across_far, downs)
+    for k in range(PLANE):
+        take_rest(k, ups)
     edge_copy(0).wait_recv()
     edge_copy(1).wait_recv()
+
+    pitch = rows + 16
     none = jnp.zeros((8, units), F32)
-    for pre, at in ((pre_g, 0), (pre_v, PLANE)):
-        after = [jnp.broadcast_to(edge_r[at + k : at + k + 1, :], (8, units)) for k in range(PLANE)]
+    for pre, held in ((pre_g, w_gate), (pre_v, w_value)):
+        both = jnp.dot(allnorm[...], held[...], preferred_element_type=F32).astype(BF).astype(F32)
+        after = [
+            jnp.broadcast_to(both[quad_rows + k : quad_rows + k + 1], (8, units))
+            for k in range(PLANE)
+        ]
         ahead = [
-            jnp.broadcast_to(edge_r[8 + at + k : 8 + at + k + 1, :], (8, units))
+            jnp.broadcast_to(both[quad_rows + 8 + k : quad_rows + 9 + k], (8, units))
             for k in range(PLANE)
         ]
         for k in range(PLANE):
+            pre[k * pitch + 8 : k * pitch + 8 + rows, :] = both[k * rows : (k + 1) * rows]
             here = k * pitch
             pre[here : here + 8, :] = jnp.where(
                 place == 0, ahead[k - 1] if k else none, ahead[k]
@@ -609,6 +700,8 @@
                 place == PLANE - 1, after[k + 1] if k + 1 < PLANE else none, after[k]
             )
 
+    unit_at = span(z * units, units, LANES)
+
     def convolve(ref, taps, k):
         block = ref[span(k * pitch, rows + 16, 8), :]
         return (
@@ -620,14 +713,17 @@
     quad = PLANE * half_rows
 
     def gated(k):
-        gate = convolve(pre_g, cg_ref, k)
-        value = convolve(pre_v, cv_ref, k)
+        gate = convolve(pre_g, cg_ref[:, unit_at], k)
+        value = convolve(pre_v, cv_ref[:, unit_at], k)
         hidden = (gate / (1.0 + jnp.exp(-gate)) * value).astype(BF)
         for c in range(2):
             hid[span(c * quad + k * half_rows, half_rows, half_rows), :] = hidden[
                 c * half_rows : (c + 1) * half_rows
             ]
 
+    take_corner(1, downs)
+    take_corner(across_far, downs)
+    take_z(5 - across_far, downs)
     loop(0, PLANE, gated)
     chunk = PLANE * LANES
 
@@ -660,9 +756,7 @@
 
     def down(c):
         take_rest(xor(z, c), downs)
-        part[c] = jnp.dot(
-            hid[...], wrecv[2 * units :, columns(c)], preferred_element_type=F32
-        ).astype(BF)
+        part[c] = nt(hid[...], w_down[columns(c), :]).astype(BF)
         dd_copy(c).start()
 
     def to_near(c):
@@ -683,33 +777,38 @@
         fin_copy(c).start()
         out_ref[mine, columns(c)] = fin_s[:, columns(c)]
 
-    take_corner(first_far, downs)
-    take_z(last_far, downs)
+    down(1)
+    take_corner(5 - across_far, downs)
+    down(2)
+    to_near(1)
     down(0)
+    to_near(2)
     down(3)
     to_near(0)
-    take_corner(last_far, downs)
+    to_far(1)
     to_near(3)
-    down(1)
+    to_far(2)
+    finish(1)
     to_far(0)
-    to_near(1)
-    down(2)
+    finish(2)
     to_far(3)
-    to_near(2)
-    to_far(1)
     finish(0)
     finish(3)
-    to_far(2)
-    finish(1)
-    finish(2)
 
     loop(1, kv_heads, lambda d: q_copy(d).wait_send())
-    for k in (2, 1, 0):
+    for e in range(PLANE):
+        kv_copy(across_far, e, True).wait_send()
+    for k in (1, 0):
         for e in range(PLANE):
             if k or e:
                 kv_copy(k, e).wait_send()
-    for e in range(PLANE):
-        kv_relay(e).wait_send()
+
+    @pl.when(inner)
+    def _():
+        for k in (2, 3):
+            for e in range(PLANE):
+                kv_relay(k, e).wait_send()
+
     for j in ups + downs:
         for k in range(PLANE):
             if k:
@@ -720,9 +819,15 @@
     loop(1, kv_heads, lambda d: o_copy(d).wait_send())
     po_copy.wait_send()
     for k in range(PLANE):
-        if k:
-            ag_copy(k).wait_send()
         fw_copy(k).wait_send()
+    ag_copy(across_far, 0).wait_send()
+    ag_copy(1, 1).wait_send()
+
+    @pl.when(inner)
+    def _():
+        ag_relay(2).wait_send()
+        ag_relay(3).wait_send()
+
     for h in range(2):
         edge_copy(h).wait_send()
     for c in range(PLANE):
@@ -735,13 +840,13 @@
 
 
 def rotary_tables(count):
-    lanes = jnp.arange(LANES)
+    lanes = np.arange(LANES)
     length = HEAD_SIZE // 2
-    rate_at = (lanes % (length // 2)).astype(F32)
-    rates = 1.0 / theta ** (rate_at * 2.0 / length)
-    angles = jnp.arange(count, dtype=F32)[:, None] * rates[None, :]
-    sign = jnp.where(lanes % length < length // 2, -1.0, 1.0)
-    return jnp.cos(angles), jnp.sin(angles) * sign[None, :]
+    rate_at = (lanes % (length // 2)).astype(np.float32)
+    rates = np.float32(1.0) / np.float32(theta) ** (rate_at * np.float32(2.0 / length))
+    angles = np.arange(count, dtype=np.float32)[:, None] * rates[None, :]
+    sign = np.where(lanes % length < length // 2, -1.0, 1.0).astype(np.float32)
+    return np.cos(angles), np.sin(angles) * sign[None, :]
 
 
 def kernel_shards(
@@ -751,16 +856,6 @@
     rows, width = x_rows.shape
     kv_heads = keys.shape[1] // HEAD_SIZE
     units = gate_weight.shape[1] // PLANE
-    depth = gate_weight.shape[0]
-    kv = jnp.concatenate(
-        [keys.reshape(rows, kv_heads, HEAD_SIZE), values.reshape(rows, kv_heads, HEAD_SIZE)], axis=-1
-    ).reshape(rows, kv_heads * LANES)
-    turned = [
-        w.T.reshape(PLANE, units, depth) for w in (gate_weight, value_weight, down_weight)
-    ]
-    weights = jnp.concatenate(turned, axis=1)
-    at = lax.axis_index("sp") // PLANE
-    taps = [lax.dynamic_slice_in_dim(t, at * units, units, 1) for t in (conv_gate, conv_value)]
     cos, sin = rotary_tables(max(GRID_ROW_WIDTH, n * rows // GRID_ROW_WIDTH))
     tokens, q_tokens, span_rows = n * rows, kv_heads * rows, PLANE * rows
     half_rows = rows // 2
@@ -768,32 +863,34 @@
     dma = pltpu.SemaphoreType.DMA
     vm = pltpu.VMEM
     padded = span_rows + 16 * PLANE
+    args = (
+        x_rows, queries, keys, values, query_norm_gain[None, :], key_norm_gain[None, :],
+        cos, sin, out_weight, ffn_gain[None, :], gate_weight, value_weight, down_weight,
+        conv_gate, conv_value,
+    )
     scratch = [
+        vm((half_rows, width), BF), vm(keys.shape, BF), vm(values.shape, BF),
+        vm((rows, kv_heads * LANES), BF), vm((1, HEAD_SIZE), F32), vm((1, HEAD_SIZE), F32),
+        vm(cos.shape, F32), vm(sin.shape, F32), vm((1, width), F32), vm(conv_gate.shape, F32),
+        vm(conv_value.shape, F32),
         vm(out_weight.shape, BF), vm((tokens, LANES), BF), vm((q_tokens, LANES), BF), vm((tokens, 2 * LANES), BF),
         vm((2 * q_tokens, LANES), BF), vm((q_tokens, LANES), BF), vm((rows, kv_heads * LANES), BF),
         vm((rows, width), BF), vm((half_rows, width), BF), vm((half_rows, width), F32),
-        vm((span_rows, width), BF), vm((16, units), F32),
-        vm((16, units), F32), vm((3 * units, width), BF),
+        vm((span_rows + 16, width), BF), vm((16, width), BF), *[vm((width, units), BF)] * 3,
         vm((padded, units), F32), vm((padded, units), F32), vm((span_rows, units), BF),
         vm((PLANE, span_rows, chunk), BF), vm((PLANE, span_rows // 2, chunk), BF),
         vm((PLANE, rows, chunk), BF), vm((PLANE, rows, chunk), BF),
         vm((PLANE, half_rows, chunk), BF), vm((PLANE, half_rows, chunk), BF),
         vm((half_rows, width), BF), vm((half_rows, width), BF),
-        dma((4,)), dma((n,)), dma((n,)), dma((kv_heads,)), dma((kv_heads,)),
+        dma((18,)), dma((n,)), dma((PLANE,)), dma((n,)), dma((kv_heads,)), dma((kv_heads,)),
         *[dma((4 * PLANE,))] * 8,
         dma((kv_heads,)), dma((kv_heads,)), dma((2,)),
         *[dma((PLANE,))] * 4, dma((2,)), dma((2,)), *[dma((PLANE,))] * 8,
     ]
-    args = (
-        x_rows, queries, kv, query_norm_gain[None, :], key_norm_gain[None, :],
-        cos, sin, out_weight, ffn_gain[None, :], weights, taps[0], taps[1],
-    )
     return pl.pallas_call(
         lambda *refs: layer_kernel(n, *refs),
         out_shape=jax.ShapeDtypeStruct((rows, width), BF),
-        in_specs=[
-            pl.BlockSpec(memory_space=pl.ANY if a is out_weight else pltpu.VMEM) for a in args
-        ],
+        in_specs=[pl.BlockSpec(memory_space=pl.ANY)] * len(args),
         out_specs=pl.BlockSpec(memory_space=pltpu.VMEM),
         scratch_shapes=scratch,
         compiler_params=pltpu.CompilerParams(

time: 143 us -> 113 us (0.79)
  Pallas kernels: 133 us -> 111 us
  local copies, waits for them, and re-layouts: 7.41 us -> 1.88 us
  other arithmetic: 2.22 us -> 0 us
    pallas_call x1, Pallas kernels: 133 us -> 111 us  [kernel_shards(): pl.pallas_call(lambda *refs: layer_kernel(n, *refs), out_shape=jax.ShapeD...]
    transpose x3 -> x0, local copies, waits for them, and re-layouts: 3.14 us -> none  [kernel_shards(): w.T.reshape(PLANE, units, depth)]
    concatenate x2 -> x0, other arithmetic: 1.44 us -> none  [the longest x1 1.43 us: kernel_shards(): weights = jnp.concatenate(turned, axis=1)]
where the time goes in v2:
time: 113 us
  Pallas kernels  111 us (98%)
  local copies, waits for them, and re-layouts  1.88 us (2%)
    pallas_call x1, Pallas kernels, kernel_shards(): pl.pallas_call(lambda *refs: layer_kernel(n, *refs), out_shape=jax.ShapeD...  111 us

profile of v2, /device:TPU:0, one launch (start us, length us, event | category | flops | bytes accessed | tf_op | source)
XLA Modules:
  0.0 113.2 jit_solution(11518242197557479690)
XLA Ops:
  0.0 111.3 %layer.1 = bf16[128,2048]{1,0:T(8,128)(2,1)} custom-call(bf16[128,2048]{1,0:T(8,128)(2,1)} %refs_0_.1, bf16[128,512]{1,0:T(8,128)(2,1)} %refs_1_.1, bf16[128,256]{1,0:T(8,128)(2,1)} %refs_2_.1, bf16[128,256]{1,0:T(8,128)(2,1)} %refs_3_.1, f32[1,64]{1,0:T(1,128)} %bitcast.4, f32[1,64]{1,0:T(1,128)} %bitcast.5, f32[64,128]{1,0:T(8,128)} %constant.4.clone.refs_6_, ...), custom_call_target="tpu_custom_call" | custom-call | tf_op jit(solution)/shard_map/layer/pallas_call | solution.py:890
  111.3 1.9 %copy.17 = bf16[128,2048]{1,0:T(8,128)(2,1)} copy(bf16[128,2048]{1,0:T(8,128)(2,1)} %layer.1) | data formatting | bytes 1048576

commit v3 on v2

--- a/solution.py
+++ b/solution.py
@@ -211,11 +211,11 @@
     n, x_hbm, q_hbm, k_hbm, v_hbm, qg_hbm, kg_hbm, cos_hbm, sin_hbm, wo_ref, fg_hbm, gate_hbm,
     value_hbm, down_hbm, cg_hbm, cv_hbm, out_ref,
     x_ref, k_ref, v_ref, kv_ref, qg_ref, kg_ref, cos_ref, sin_ref, fg_ref, cg_ref, cv_ref,
-    wo_buf, kvbuf, qbuf, kcat, qcat, att_s, attbuf, po_s, po_r, mid, allnorm, edge_s, w_gate, w_value, w_down,
-    pre_g, pre_v, hid, part, ddbuf, near_s, near_r, far_s, far_r, fin_s, fin_r,
+    wo_buf, kvbuf, qbuf, kcat, qcat, att_s, attbuf, po_s, po_r, mid, allnorm, edge_s, edge_r, w_gate, w_value, w_down,
+    pre_g, pre_v, hid, part, ddbuf, near_s, near_r, far_s, far_r, fin_s,
     loc, kv_ss, kf_ss, kv_rs, q_ss, q_rs, s1_ss, s1_rs, x_ss, x_rs, y_ss, y_rs, d_ss, d_rs, o_ss, o_rs,
-    po_sem, ag_ss, ag_rs, fw_ss, fw_rs, h_ss, h_rs, dd_ss, dd_rs, near_ss, near_rs, far_ss, far_rs,
-    fin_ss, fin_rs,
+    po_sem, ag_ss, ag_rs, fw_ss, fw_rs, h_ss, h_rs, e_sem, dd_ss, dd_rs, near_ss, near_rs, far_ss, far_rs,
+    fin_ss, fin_rs, out_sem,
 ):
     sp = lax.axis_index("sp")
     core = lax.axis_index("tp")
@@ -397,10 +397,9 @@
         for j in ups:
             by_z(k, j).start()
 
-    def far_down():
-        for k in (3, 2):
-            for j in downs:
-                by_z(k, j).start()
+    def far_down(k):
+        for j in downs:
+            by_z(k, j).start()
 
     loop(1, kv_heads, lambda d: q_copy(d).start())
     for e in range(PLANE):
@@ -419,7 +418,7 @@
         for j in downs:
             by_z(1, j).start()
 
-    pl.when(outer)(near_up)
+    near_up()
     far_up(across_far)
 
     @pl.when(outer)
@@ -517,9 +516,12 @@
 
         @pl.when(jnp.logical_and(inner, i == 3 * PLANE - 1))
         def _():
-            near_up()
             far_up(2)
             near_down()
+
+        @pl.when(jnp.logical_and(outer, i == 2 * PLANE))
+        def _():
+            take_z(1, ups)
 
         @pl.when(jnp.logical_and(outer, i == 3 * PLANE))
         def _():
@@ -595,19 +597,41 @@
     mid[...] = middle
     scaled = lax.rsqrt(jnp.mean(middle * middle, axis=1, keepdims=True) + eps_norm)
     normed = (middle * scaled * fg_ref[...]).astype(BF)
+    tall = 2 * rows + 16
 
     def slot(k, c):
-        return allnorm.at[span(xor(z, k) * rows + c * half_rows, half_rows, half_rows)]
-
-    allnorm[span(z * rows + core * half_rows, half_rows, half_rows), :] = normed
+        base = (tall, 0)[k] if isinstance(k, int) and k < 2 else rows + (3 - k) * tall
+        return allnorm.at[span(base + c * half_rows, half_rows, 16)]
+
+    slot(0, core)[...] = normed
+    wide = normed.astype(F32)
+    outermost = jnp.where(core == 0, wide[:1], wide[half_rows - 1 :])
+    edge_s[...] = jnp.concatenate(
+        [outermost[:, b * LANES : (b + 1) * LANES] for b in range(width // LANES)], axis=0
+    ).astype(BF)
+
+    def edge_copy(k):
+        to = xor(z, k) * PLANE + rem(place + jnp.where(core == 0, PLANE - 1, 1), PLANE)
+        return remote(
+            edge_s, edge_r.at[core * PLANE + z], h_ss.at[k], h_rs.at[z], (to, core)
+        )
+
+    def edge_share(side):
+        at = edge_r.at[pl.ds(side * PLANE, PLANE)]
+        return remote(at, at, e_sem.at[0], e_sem.at[1], (sp, mate))
+
+    for k in range(PLANE):
+        edge_copy(k).start()
 
     def ag_copy(k, i):
-        at = slot(0, core)
-        return remote(at, at, ag_ss.at[i], ag_rs.at[k], (chip(k, 0), core))
+        return remote(
+            slot(0, core), slot(k, core), ag_ss.at[i], ag_rs.at[k], (chip(k, 0), core)
+        )
 
     def ag_relay(k):
-        at = slot(k, core)
-        return remote(at, at, ag_ss.at[5 - k], ag_rs.at[5 - k], (chip(1, 0), core))
+        return remote(
+            slot(k, core), slot(5 - k, core), ag_ss.at[5 - k], ag_rs.at[5 - k], (chip(1, 0), core)
+        )
 
     def fw_copy(k):
         at = slot(k, core)
@@ -623,82 +647,74 @@
     ag_copy(across_far, 0).start()
     ag_copy(1, 1).start()
     fw_copy(0).start()
-    pl.when(inner)(far_down)
+    pl.when(inner)(lambda: far_down(3))
+    pl.when(inner)(lambda: far_down(2))
     take_corner(0, downs)
-    pl.when(outer)(lambda: take_z(1, ups))
     take_corner(1, ups)
+    pl.when(outer)(lambda: far_down(2))
     pl.when(outer)(lambda: take_z(3, ups))
-
-    @pl.when(inner)
-    def _():
-        take_z(2, ups)
-        take_corner(3, ups)
-        ag_take(first_far)
-        take_corner(2, ups)
-
-    @pl.when(outer)
-    def _():
-        take_z(2, ups)
-        take_corner(3, ups)
-        take_corner(2, ups)
-        far_down()
-        ag_take(first_far)
-
+    pl.when(outer)(lambda: take_z(1, downs))
+    pl.when(inner)(lambda: take_z(2, ups))
+    pl.when(inner)(lambda: take_corner(3, ups))
+    pl.when(inner)(lambda: ag_take(first_far))
+    pl.when(inner)(lambda: take_corner(2, ups))
+    pl.when(outer)(lambda: take_z(2, ups))
+    pl.when(outer)(lambda: take_corner(3, ups))
+    pl.when(outer)(lambda: ag_take(first_far))
+    pl.when(outer)(lambda: far_down(3))
+    pl.when(outer)(lambda: take_corner(2, ups))
+    pl.when(inner)(lambda: take_z(1, downs))
+    pl.when(inner)(lambda: take_z(2, downs))
     ag_take(1)
-    ag_take(last_far)
+    for k in range(PLANE):
+        at = edge_r.at[core * PLANE + k]
+        remote(at, at, h_ss.at[k], h_rs.at[k], (sp, mate)).wait_recv()
+    edge_share(core).start()
+    pl.when(inner)(lambda: ag_take(last_far))
     for copy in own_w:
         copy.wait()
-    for k in range(PLANE):
-        at = slot(k, mate)
-        remote(at, at, fw_ss.at[k], fw_rs.at[k], (sp, mate)).wait_recv()
-    quad_rows = PLANE * rows
-    edge_s[...] = jnp.concatenate(
-        [
-            allnorm[k * rows + at : k * rows + at + 1, :]
-            for at in (0, rows - 1)
-            for k in tuple(range(PLANE)) * (8 // PLANE)
-        ],
-        axis=0,
-    )
-
-    def edge_copy(h):
-        at = slice(8 * h, 8 * h + 8)
-        to = q_base + rem(place + (PLANE - 1, 1)[h], PLANE)
-        return remote(
-            edge_s.at[at], allnorm.at[quad_rows + 8 * h : quad_rows + 8 * h + 8],
-            h_ss.at[h], h_rs.at[h], (to, core),
-        )
-
-    edge_copy(0).start()
-    edge_copy(1).start()
-    take_z(1, downs)
-    take_z(across_far, downs)
+
+    def mate_take(ks):
+        for k in ks:
+            at = slot(k, mate)
+            remote(at, at, fw_ss.at[k], fw_rs.at[k], (sp, mate)).wait_recv()
+
+    def edge_row(side, at):
+        inside = jnp.logical_and(at >= 0, at < PLANE)
+        tile = edge_r[side * PLANE + jnp.where(inside, at, 0)].astype(F32)
+        row = jnp.concatenate([tile[b : b + 1] for b in range(width // LANES)], axis=1)
+        return jnp.where(inside, row, 0.0)
+
+    halves = ((1, 3), (0, 2))
+    mate_take(halves[0])
+    edge_share(mate).wait_recv()
+    for h in range(2):
+        ends = []
+        for k in halves[h]:
+            ends.append(edge_row(1, xor(z, k) - jnp.where(place == 0, 1, 0)))
+            ends.append(edge_row(0, xor(z, k) + jnp.where(place == PLANE - 1, 1, 0)))
+        allnorm[h * tall + 2 * rows : (h + 1) * tall, :] = jnp.concatenate(
+            ends * 4, axis=0
+        ).astype(BF)
+    take_corner(1, downs)
     for k in range(PLANE):
         take_rest(k, ups)
-    edge_copy(0).wait_recv()
-    edge_copy(1).wait_recv()
 
     pitch = rows + 16
-    none = jnp.zeros((8, units), F32)
-    for pre, held in ((pre_g, w_gate), (pre_v, w_value)):
-        both = jnp.dot(allnorm[...], held[...], preferred_element_type=F32).astype(BF).astype(F32)
-        after = [
-            jnp.broadcast_to(both[quad_rows + k : quad_rows + k + 1], (8, units))
-            for k in range(PLANE)
-        ]
-        ahead = [
-            jnp.broadcast_to(both[quad_rows + 8 + k : quad_rows + 9 + k], (8, units))
-            for k in range(PLANE)
-        ]
-        for k in range(PLANE):
-            pre[k * pitch + 8 : k * pitch + 8 + rows, :] = both[k * rows : (k + 1) * rows]
-            here = k * pitch
-            pre[here : here + 8, :] = jnp.where(
-                place == 0, ahead[k - 1] if k else none, ahead[k]
+
+    def up(h):
+        for pre, held in ((pre_g, w_gate), (pre_v, w_value)):
+            both = jnp.dot(
+                allnorm[h * tall : (h + 1) * tall, :], held[...], preferred_element_type=F32
             )
-            pre[here + 8 + rows : here + pitch, :] = jnp.where(
-                place == PLANE - 1, after[k + 1] if k + 1 < PLANE else none, after[k]
-            )
+            both = both.astype(BF).astype(F32)
+            for b in range(2):
+                here, end = (2 * h + b) * pitch, 2 * rows + 2 * b
+                pre[here + 8 : here + 8 + rows, :] = both[b * rows : (b + 1) * rows]
+                pre[here : here + 8, :] = jnp.broadcast_to(both[end : end + 1], (8, units))
+                pre[here + 8 + rows : here + pitch, :] = jnp.broadcast_to(
+                    both[end + 1 : end + 2], (8, units)
+                )
 
     unit_at = span(z * units, units, LANES)
 
@@ -710,30 +726,23 @@
             + taps[2:3, :] * block[9 : 9 + rows]
         )
 
-    quad = PLANE * half_rows
-
     def gated(k):
         gate = convolve(pre_g, cg_ref[:, unit_at], k)
         value = convolve(pre_v, cv_ref[:, unit_at], k)
         hidden = (gate / (1.0 + jnp.exp(-gate)) * value).astype(BF)
         for c in range(2):
-            hid[span(c * quad + k * half_rows, half_rows, half_rows), :] = hidden[
-                c * half_rows : (c + 1) * half_rows
-            ]
-
-    take_corner(1, downs)
-    take_corner(across_far, downs)
-    take_z(5 - across_far, downs)
-    loop(0, PLANE, gated)
+            at = (k // 2) * 2 * rows + c * rows + rem(k, 2) * half_rows
+            hid[span(at, half_rows, half_rows), :] = hidden[c * half_rows : (c + 1) * half_rows]
+
     chunk = PLANE * LANES
 
     def columns(c):
-        return slice(c * chunk, (c + 1) * chunk)
-
-    def dd_copy(c):
+        return span(c * chunk, chunk, chunk)
+
+    def dd_copy(c, h):
         return remote(
-            part.at[c, span(mate * quad, quad, quad)], ddbuf.at[c], dd_ss.at[c], dd_rs.at[c],
-            (sp, mate),
+            part.at[c, h, span(mate * rows, rows, rows)], ddbuf.at[c, h],
+            dd_ss.at[2 * c + h], dd_rs.at[2 * c + h], (sp, mate),
         )
 
     def near_copy(c):
@@ -744,56 +753,83 @@
 
     def fin_copy(c):
         return remote(
-            fin_s.at[:, columns(c)], fin_r.at[:, columns(c)], fin_ss.at[c], fin_rs.at[c], (sp, mate)
-        )
-
-    def summed_for(c, k):
-        at = xor(z, k) * half_rows
-        return (
-            part[c, span(core * quad + at, half_rows, half_rows), :].astype(F32)
-            + ddbuf[c, span(at, half_rows, half_rows), :].astype(F32)
-        )
-
-    def down(c):
-        take_rest(xor(z, c), downs)
-        part[c] = nt(hid[...], w_down[columns(c), :]).astype(BF)
-        dd_copy(c).start()
+            fin_s.at[:, columns(c)], out_ref.at[mine, columns(c)], fin_ss.at[c], fin_rs.at[c],
+            (sp, mate),
+        )
+
+    def out_copy(c):
+        return pltpu.make_async_copy(
+            fin_s.at[:, columns(c)], out_ref.at[mine, columns(c)], out_sem.at[c]
+        )
+
+    theirs = span(mate * half_rows, half_rows, half_rows)
+
+    def fin_take(c):
+        at = out_ref.at[theirs, columns(c)]
+        remote(at, at, fin_ss.at[c], fin_rs.at[c], (sp, mate)).wait_recv()
+
+    def summed(c, h):
+        return part[c, h, span(core * rows, rows, rows), :].astype(F32) + ddbuf[c, h].astype(F32)
+
+    def down(c, h):
+        if h == 0:
+            take_rest(xor(z, c), downs)
+        part[c, h] = nt(hid[2 * h * rows : 2 * (h + 1) * rows, :], w_down[columns(c), :]).astype(BF)
+        dd_copy(c, h).start()
 
     def to_near(c):
-        dd_copy(c).wait_recv()
-        near_s[c, :half_rows, :] = summed_for(c, 1).astype(BF)
-        near_s[c, half_rows:, :] = summed_for(c, 3).astype(BF)
+        dd_copy(c, 0).wait_recv()
+        near_s[c] = summed(c, 0).astype(BF)
         near_copy(c).start()
 
     def to_far(c):
         near_copy(c).wait_recv()
-        far_s[c] = (summed_for(c, 2) + near_r[c, half_rows:, :].astype(F32)).astype(BF)
+        dd_copy(c, 1).wait_recv()
+        both = summed(c, 1) + near_r[c].astype(F32)
+        far_s[c] = both[half_rows:].astype(BF)
         far_copy(c).start()
+        mid[:, columns(c)] = mid[:, columns(c)] + both[:half_rows]
 
     def finish(c):
-        ours = mid[:, columns(c)] + summed_for(c, 0) + near_r[c, :half_rows, :].astype(F32)
         far_copy(c).wait_recv()
-        fin_s[:, columns(c)] = (ours + far_r[c].astype(F32)).astype(BF)
+        fin_s[:, columns(c)] = (mid[:, columns(c)] + far_r[c].astype(F32)).astype(BF)
         fin_copy(c).start()
-        out_ref[mine, columns(c)] = fin_s[:, columns(c)]
-
-    down(1)
+        out_copy(c).start()
+
+    lower = z < PLANE // 2
+    c0, c1, c2, c3 = [jnp.where(lower, a, b) for a, b in ((0, 2), (1, 3), (3, 0), (2, 1))]
+    up(0)
+    pl.when(outer)(lambda: ag_take(last_far))
+    pl.when(outer)(lambda: take_z(3, downs))
+    take_z(across_far, downs)
+    loop(0, 2, gated)
+    down(c0, 0)
+    down(c1, 0)
+    to_near(c0)
+    to_near(c1)
     take_corner(5 - across_far, downs)
-    down(2)
-    to_near(1)
-    down(0)
-    to_near(2)
-    down(3)
-    to_near(0)
-    to_far(1)
-    to_near(3)
-    to_far(2)
-    finish(1)
-    to_far(0)
-    finish(2)
-    to_far(3)
-    finish(0)
-    finish(3)
+    mate_take(halves[1])
+    up(1)
+    take_corner(across_far, downs)
+    loop(2, 4, gated)
+    down(c0, 1)
+    down(c1, 1)
+    pl.when(outer)(lambda: to_far(c0))
+    pl.when(outer)(lambda: to_far(c1))
+    down(c2, 0)
+    to_near(c2)
+    down(c2, 1)
+    pl.when(inner)(lambda: to_far(c0))
+    pl.when(inner)(lambda: to_far(c1))
+    down(c3, 0)
+    to_near(c3)
+    down(c3, 1)
+    to_far(c2)
+    finish(c2)
+    to_far(c3)
+    finish(c3)
+    finish(c0)
+    finish(c1)
 
     loop(1, kv_heads, lambda d: q_copy(d).wait_send())
     for e in range(PLANE):
@@ -828,15 +864,17 @@
         ag_relay(2).wait_send()
         ag_relay(3).wait_send()
 
-    for h in range(2):
-        edge_copy(h).wait_send()
+    for k in range(PLANE):
+        edge_copy(k).wait_send()
+    edge_share(core).wait_send()
     for c in range(PLANE):
-        dd_copy(c).wait_send()
+        dd_copy(c, 0).wait_send()
+        dd_copy(c, 1).wait_send()
         near_copy(c).wait_send()
         far_copy(c).wait_send()
         fin_copy(c).wait_send()
-        fin_copy(c).wait_recv()
-    out_ref[span(mate * half_rows, half_rows, half_rows), :] = fin_r[...]
+        out_copy(c).wait()
+        fin_take(c)
 
 
 def rotary_tables(count):
@@ -876,22 +914,23 @@
         vm(out_weight.shape, BF), vm((tokens, LANES), BF), vm((q_tokens, LANES), BF), vm((tokens, 2 * LANES), BF),
         vm((2 * q_tokens, LANES), BF), vm((q_tokens, LANES), BF), vm((rows, kv_heads * LANES), BF),
         vm((rows, width), BF), vm((half_rows, width), BF), vm((half_rows, width), F32),
-        vm((span_rows + 16, width), BF), vm((16, width), BF), *[vm((width, units), BF)] * 3,
+        vm((span_rows + 32, width), BF), vm((width // LANES, LANES), BF),
+        vm((2 * PLANE, width // LANES, LANES), BF), *[vm((width, units), BF)] * 3,
         vm((padded, units), F32), vm((padded, units), F32), vm((span_rows, units), BF),
-        vm((PLANE, span_rows, chunk), BF), vm((PLANE, span_rows // 2, chunk), BF),
+        vm((PLANE, 2, 2 * rows, chunk), BF), vm((PLANE, 2, rows, chunk), BF),
         vm((PLANE, rows, chunk), BF), vm((PLANE, rows, chunk), BF),
         vm((PLANE, half_rows, chunk), BF), vm((PLANE, half_rows, chunk), BF),
-        vm((half_rows, width), BF), vm((half_rows, width), BF),
+        vm((half_rows, width), BF),
         dma((18,)), dma((n,)), dma((PLANE,)), dma((n,)), dma((kv_heads,)), dma((kv_heads,)),
         *[dma((4 * PLANE,))] * 8,
         dma((kv_heads,)), dma((kv_heads,)), dma((2,)),
-        *[dma((PLANE,))] * 4, dma((2,)), dma((2,)), *[dma((PLANE,))] * 8,
+        *[dma((PLANE,))] * 6, dma((2,)), dma((2 * PLANE,)), dma((2 * PLANE,)), *[dma((PLANE,))] * 7,
     ]
     return pl.pallas_call(
         lambda *refs: layer_kernel(n, *refs),
         out_shape=jax.ShapeDtypeStruct((rows, width), BF),
         in_specs=[pl.BlockSpec(memory_space=pl.ANY)] * len(args),
-        out_specs=pl.BlockSpec(memory_space=pltpu.VMEM),
+        out_specs=pl.BlockSpec(memory_space=pl.ANY),
         scratch_shapes=scratch,
         compiler_params=pltpu.CompilerParams(
             collective_id=0, has_side_effects=True, vmem_limit_bytes=60 * 2**20

time: 113 us -> 103 us (0.912)
  Pallas kernels: 111 us -> 101 us
    pallas_call x1, Pallas kernels: 111 us -> 101 us  [kernel_shards(): pl.pallas_call(lambda *refs: layer_kernel(n, *refs), out_shape=jax.ShapeD...]
where the time goes in v3:
time: 103 us; the launch traced here: 102 us
  Pallas kernels  101 us (98%)
  local copies, waits for them, and re-layouts  1.88 us (2%)
    pallas_call x1, Pallas kernels, kernel_shards(): pl.pallas_call(lambda *refs: layer_kernel(n, *refs), out_shape=jax.ShapeD...  101 us

profile of v3, /device:TPU:0, one launch (start us, length us, event | category | flops | bytes accessed | tf_op | source)
XLA Modules:
  0.0 102.4 jit_solution(17799715453479077405)
XLA Ops:
  0.0 100.5 %layer.1 = bf16[128,2048]{1,0:T(8,128)(2,1)} custom-call(bf16[128,2048]{1,0:T(8,128)(2,1)} %refs_0_.1, bf16[128,512]{1,0:T(8,128)(2,1)} %refs_1_.1, bf16[128,256]{1,0:T(8,128)(2,1)} %refs_2_.1, bf16[128,256]{1,0:T(8,128)(2,1)} %refs_3_.1, f32[1,64]{1,0:T(1,128)} %bitcast.4, f32[1,64]{1,0:T(1,128)} %bitcast.5, f32[64,128]{1,0:T(8,128)} %constant.4.clone.refs_6_, ...), custom_call_target="tpu_custom_call" | custom-call | tf_op jit(solution)/shard_map/layer/pallas_call | solution.py:929
  100.5 1.9 %copy.17 = bf16[128,2048]{1,0:T(8,128)(2,1)} copy(bf16[128,2048]{1,0:T(8,128)(2,1)} %layer.1) | data formatting | bytes 1048576

commit v4 on v3

--- a/solution.py
+++ b/solution.py
@@ -215,7 +215,7 @@
     pre_g, pre_v, hid, part, ddbuf, near_s, near_r, far_s, far_r, fin_s,
     loc, kv_ss, kf_ss, kv_rs, q_ss, q_rs, s1_ss, s1_rs, x_ss, x_rs, y_ss, y_rs, d_ss, d_rs, o_ss, o_rs,
     po_sem, ag_ss, ag_rs, fw_ss, fw_rs, h_ss, h_rs, e_sem, dd_ss, dd_rs, near_ss, near_rs, far_ss, far_rs,
-    fin_ss, fin_rs, out_sem,
+    fin_ss, fin_rs,
 ):
     sp = lax.axis_index("sp")
     core = lax.axis_index("tp")
@@ -527,7 +527,7 @@
         def _():
             take_corner(0, ups)
 
-        @pl.when(i == PLANE)
+        @pl.when(i == 1)
         def _():
             spread(0, ups)
             spread(0, downs)
@@ -757,11 +757,6 @@
             (sp, mate),
         )
 
-    def out_copy(c):
-        return pltpu.make_async_copy(
-            fin_s.at[:, columns(c)], out_ref.at[mine, columns(c)], out_sem.at[c]
-        )
-
     theirs = span(mate * half_rows, half_rows, half_rows)
 
     def fin_take(c):
@@ -794,7 +789,7 @@
         far_copy(c).wait_recv()
         fin_s[:, columns(c)] = (mid[:, columns(c)] + far_r[c].astype(F32)).astype(BF)
         fin_copy(c).start()
-        out_copy(c).start()
+        out_ref[mine, columns(c)] = fin_s[:, columns(c)]
 
     lower = z < PLANE // 2
     c0, c1, c2, c3 = [jnp.where(lower, a, b) for a, b in ((0, 2), (1, 3), (3, 0), (2, 1))]
@@ -873,7 +868,6 @@
         near_copy(c).wait_send()
         far_copy(c).wait_send()
         fin_copy(c).wait_send()
-        out_copy(c).wait()
         fin_take(c)
 
 
@@ -924,13 +918,13 @@
         dma((18,)), dma((n,)), dma((PLANE,)), dma((n,)), dma((kv_heads,)), dma((kv_heads,)),
         *[dma((4 * PLANE,))] * 8,
         dma((kv_heads,)), dma((kv_heads,)), dma((2,)),
-        *[dma((PLANE,))] * 6, dma((2,)), dma((2 * PLANE,)), dma((2 * PLANE,)), *[dma((PLANE,))] * 7,
+        *[dma((PLANE,))] * 6, dma((2,)), dma((2 * PLANE,)), dma((2 * PLANE,)), *[dma((PLANE,))] * 6,
     ]
     return pl.pallas_call(
         lambda *refs: layer_kernel(n, *refs),
-        out_shape=jax.ShapeDtypeStruct((rows, width), BF),
+        out_shape=pltpu.VMEM((rows, width), BF),
         in_specs=[pl.BlockSpec(memory_space=pl.ANY)] * len(args),
-        out_specs=pl.BlockSpec(memory_space=pl.ANY),
+        out_specs=pl.BlockSpec(memory_space=pltpu.VMEM),
         scratch_shapes=scratch,
         compiler_params=pltpu.CompilerParams(
             collective_id=0, has_side_effects=True, vmem_limit_bytes=60 * 2**20

time: 103 us -> 100 us (0.971)
  Pallas kernels: 101 us -> 99.4 us
  local copies, waits for them, and re-layouts: 1.88 us -> 0.8 us
    unnamed x1, local copies, waits for them, and re-layouts: 1.88 us -> 0.8 us
    pallas_call x1, Pallas kernels: 101 us -> 99.4 us  [kernel_shards(): pl.pallas_call(lambda *refs: layer_kernel(n, *refs), out_shape=pltpu.VMEM...]
where the time goes in v4:
time: 100 us
  Pallas kernels  99.4 us (99%)
    pallas_call x1, Pallas kernels, kernel_shards(): pl.pallas_call(lambda *refs: layer_kernel(n, *refs), out_shape=pltpu.VMEM...  99.4 us

profile of v4, /device:TPU:0, one launch (start us, length us, event | category | flops | bytes accessed | tf_op | source)
XLA Modules:
  0.0 100.3 jit_solution(15234047045589064867)
XLA Ops:
  0.0 99.4 %layer.1 = bf16[128,2048]{1,0:T(8,128)(2,1)S(1)} custom-call(bf16[128,2048]{1,0:T(8,128)(2,1)} %refs_0_.1, bf16[128,512]{1,0:T(8,128)(2,1)} %refs_1_.1, bf16[128,256]{1,0:T(8,128)(2,1)} %refs_2_.1, bf16[128,256]{1,0:T(8,128)(2,1)} %refs_3_.1, f32[1,64]{1,0:T(1,128)} %bitcast.4, f32[1,64]{1,0:T(1,128)} %bitcast.5, f32[64,128]{1,0:T(8,128)} %constant.4.clone.refs_6_, ...), custom_call_target="tpu_custom_call" | custom-call | tf_op jit(solution)/shard_map/layer/pallas_call | solution.py:923
  99.5 0.8 copy.17

commit v5 on v4

--- a/solution.py
+++ b/solution.py
@@ -426,6 +426,7 @@
         far_up(3)
         near_down()
 
+    spread(0, ups)
     own_kv.start()
     for copy in own_w:
         copy.start()
@@ -529,7 +530,6 @@
 
         @pl.when(i == 1)
         def _():
-            spread(0, ups)
             spread(0, downs)
 
         for r in range(steps):

time: 100 us -> 99.7 us (level)
  no operation moved by 1% of the time
where the time goes in v5:
time: 99.7 us; the launch traced here: 99.5 us
  Pallas kernels  98.7 us (99%)
    pallas_call x1, Pallas kernels, kernel_shards(): pl.pallas_call(lambda *refs: layer_kernel(n, *refs), out_shape=pltpu.VMEM...  98.7 us

profile of v5, /device:TPU:0, one launch (start us, length us, event | category | flops | bytes accessed | tf_op | source)
XLA Modules:
  0.0 99.5 jit_solution(17948297253217894402)
XLA Ops:
  0.0 98.7 %layer.1 = bf16[128,2048]{1,0:T(8,128)(2,1)S(1)} custom-call(bf16[128,2048]{1,0:T(8,128)(2,1)} %refs_0_.1, bf16[128,512]{1,0:T(8,128)(2,1)} %refs_1_.1, bf16[128,256]{1,0:T(8,128)(2,1)} %refs_2_.1, bf16[128,256]{1,0:T(8,128)(2,1)} %refs_3_.1, f32[1,64]{1,0:T(1,128)} %bitcast.4, f32[1,64]{1,0:T(1,128)} %bitcast.5, f32[64,128]{1,0:T(8,128)} %constant.4.clone.refs_6_, ...), custom_call_target="tpu_custom_call" | custom-call | tf_op jit(solution)/shard_map/layer/pallas_call | solution.py:923
  98.7 0.8 copy.17
